TPU v7x, 32 devices: a whole 2x2x4 slice. The times are simulated.
32 devices in a mesh: ep: 8 (over z, core), tp: 4 (over y, x).
Axes of the slice: x: 2, y: 2, z: 4, core: 2. Of those that a mesh axis runs over, the one named last changes fastest.
Arguments:
- q_latent: bfloat16 [1536, 512], P('ep'), may hold values from -6 to 6
- kv_latent: bfloat16 [1536, 256], P('ep'), may hold values from -6 to 6
- rope_key: bfloat16 [1536, 64], P('ep'), may hold values from -900 to 900
- q_gain: float32 [512], replicated, may hold values from 0.1 to 1.9
- kv_gain: float32 [256], replicated, may hold values from 0.1 to 1.9
- w_query: bfloat16 [512, 3072], P(None, 'tp'), may hold values from -0.25 to 0.25
- w_key: bfloat16 [256, 2048], P(None, 'tp'), may hold values from -0.375 to 0.375
- w_value: bfloat16 [256, 2048], P(None, 'tp'), may hold values from -0.375 to 0.375
- w_mix_out: bfloat16 [2048, 2048], P('tp'), may hold values from -0.125 to 0.125
- expert_in: bfloat16 [1024, 2048], P('ep'), may hold values from -6 to 6
- norm_gain: float32 [2048], replicated, may hold values from 0.1 to 1.9
- routes: int32 [1024, 2], P('ep'), may hold values from 0 to 7, all different within a row; in each aligned block of 128 rows (0 to 127, 128 to 255, ...) at most 64 rows name the same one
- route_scores: float32 [1024, 2], P('ep'), may hold values from 0.05 to 1
- w_gate: bfloat16 [8, 2048, 4096], P('ep', None, 'tp'), may hold values from -0.125 to 0.125
- w_up: bfloat16 [8, 2048, 4096], P('ep', None, 'tp'), may hold values from -0.125 to 0.125
- w_down: bfloat16 [8, 4096, 2048], P('ep', 'tp'), may hold values from -0.125 to 0.125
Outputs:
- mixed: bfloat16 [1536, 2048], P(('ep', 'tp'))
- expert_out: bfloat16 [1024, 2048], P('ep', 'tp')
Inputs may be any that keep to these rules, and one draw needn't show every extreme that they name: `routes`: each row names 2 different experts; in the rows of one index of ep no expert is named by more than 64 rows, a bound that some block reaches.
All inputs are finite; a program needn't handle non-finite values.
Results may differ from a plain program's by a relative error of at most 0.03.
The roundings to bfloat16 on the way count: a program that leaves them out, or rounds other values in their place, can miss the bound.
Values may be sent and summed in bfloat16 or wider, within the bound.
A program may use at most 64 MiB of HBM per device.

v0:
```python
import functools

import jax
import jax.numpy as jnp
from jax import lax
from jax.experimental import pallas as pl
from jax.experimental.pallas import tpu as pltpu
from jax.sharding import PartitionSpec as P

NOPE = 128
ROPE = 64
VDIM = 128


eps_norm = 1e-05
rope_base = 10000.0


MESH = pl.DeviceIdType.MESH


def remote(src, dst, send, recv, ep, tp):
    return pltpu.make_async_remote_copy(
        src_ref=src, dst_ref=dst, send_sem=send, recv_sem=recv, device_id=(ep, tp), device_id_type=MESH
    )


def greet(ep_size, tp_size, me, part):
    barrier = pltpu.get_barrier_semaphore()
    for d in range(1, ep_size):
        pl.semaphore_signal(
            barrier, inc=1, device_id=(lax.rem(me + d, ep_size), part), device_id_type=MESH
        )
    for k in range(1, tp_size):
        pl.semaphore_signal(
            barrier, inc=1, device_id=(me, lax.rem(part + k, tp_size)), device_id_type=MESH
        )
    pl.semaphore_wait(barrier, ep_size + tp_size - 2)


def gather_kernel(
    ep_size, tp_size, kv, tok, tab, okv, otok, otab,
    z_send, z_recv, t_send, t_recv, c_send, c_recv, o_send, o_recv, b_send, b_recv, local,
):
    me = lax.axis_index("ep")
    part = lax.axis_index("tp")
    levels = ep_size // 2
    level, core = me // 2, me % 2
    twin = level * 2 + 1 - core
    greet(ep_size, tp_size, me, part)
    pairs = ((kv, okv), (tok, otok))
    waits = []
    own = [pltpu.make_async_copy(tab.at[me], otab.at[me], local.at[2])]
    for a, (src, dst) in enumerate(pairs):
        own.append(pltpu.make_async_copy(src, dst.at[me], local.at[a]))
    for copy in own:
        copy.start()
    order = [d for d in range(1, levels)]
    for a, (src, dst) in enumerate(pairs):
        for d in order:
            target = lax.rem(level + d, levels) * 2 + core
            copy = remote(
                src.at[part], dst.at[me, part], z_send.at[a, d], z_recv.at[a, d], target, part
            )
            copy.start()
            waits.append(copy)
        if a == 0:
            for d in range(1, ep_size):
                target = lax.rem(me + d, ep_size)
                copy = remote(
                    tab.at[target], otab.at[me], b_send.at[d], b_recv.at[d], target, part
                )
                copy.start()
                waits.append(copy)
    for a, (src, dst) in enumerate(pairs):
        copy = remote(src, dst.at[me], o_send.at[a], o_recv.at[a], twin, part)
        copy.start()
        waits.append(copy)
    for a, (src, dst) in enumerate(pairs):
        for d in order:
            block = lax.rem(level - d + levels, levels) * 2 + core
            here = dst.at[block, part]
            remote(here, here, z_send.at[a, d], z_recv.at[a, d], twin, part).wait_recv()
            for k in range(1, tp_size):
                copy = remote(
                    here, here, t_send.at[a, d, k], t_recv.at[a, d, k],
                    me, lax.rem(part + k, tp_size),
                )
                copy.start()
                waits.append(copy)
            copy = remote(here, here, c_send.at[a, d, 0], c_recv.at[a, d, 0], twin, part)
            copy.start()
            waits.append(copy)
    for a, (src, dst) in enumerate(pairs):
        for d in order:
            block = lax.rem(level - d + levels, levels) * 2 + core
            for k in range(1, tp_size):
                here = dst.at[block, lax.rem(part - k + tp_size, tp_size)]
                remote(here, here, t_send.at[a, d, k], t_recv.at[a, d, k], twin, part).wait_recv()
                copy = remote(here, here, c_send.at[a, d, k], c_recv.at[a, d, k], twin, part)
                copy.start()
                waits.append(copy)
    for a, (src, dst) in enumerate(pairs):
        remote(src, dst.at[twin], o_send.at[a], o_recv.at[a], twin, part).wait_recv()
        for d in order:
            block = lax.rem(level - d + levels, levels) * 2 + 1 - core
            for k in range(tp_size):
                here = dst.at[block, lax.rem(part - k + tp_size, tp_size)]
                remote(here, here, c_send.at[a, d, k], c_recv.at[a, d, k], twin, part).wait_recv()
    for d in range(1, ep_size):
        source = lax.rem(me - d + ep_size, ep_size)
        here = otab.at[source]
        remote(here, here, b_send.at[d], b_recv.at[d], twin, part).wait_recv()
    for copy in waits:
        copy.wait_send()
    for copy in own:
        copy.wait()


def vmem(count):
    return [pl.BlockSpec(memory_space=pltpu.VMEM)] * count


def gather_all(kv, tok, tab):
    ep_size, tp_size = lax.axis_size("ep"), lax.axis_size("tp")
    levels = ep_size // 2
    dma = pltpu.SemaphoreType.DMA
    return pl.pallas_call(
        functools.partial(gather_kernel, ep_size, tp_size),
        out_shape=(
            jax.ShapeDtypeStruct((ep_size,) + kv.shape, kv.dtype),
            jax.ShapeDtypeStruct((ep_size,) + tok.shape, tok.dtype),
            jax.ShapeDtypeStruct(tab.shape, tab.dtype),
        ),
        in_specs=vmem(3),
        out_specs=tuple(vmem(3)),
        scratch_shapes=[
            dma((2, levels)), dma((2, levels)),
            dma((2, levels, tp_size)), dma((2, levels, tp_size)),
            dma((2, levels, tp_size)), dma((2, levels, tp_size)),
            dma((2,)), dma((2,)), dma((ep_size,)), dma((ep_size,)), dma((3,)),
        ],
        compiler_params=pltpu.CompilerParams(
            collective_id=0, has_side_effects=True, vmem_limit_bytes=60 * 1024 * 1024
        ),
    )(kv, tok, tab)


def reduce_kernel(
    ep_size, tp_size, part_ref, mix, comb, mixed, landed, mix_landed, reduced,
    p_send, p_recv, m_send, m_recv, r_send, r_recv, local,
):
    me = lax.axis_index("ep")
    part = lax.axis_index("tp")
    greet(ep_size, tp_size, me, part)
    features = comb.shape[2]
    waits = []

    def columns(index):
        return pl.ds(pl.multiple_of(index * features, features), features)

    order = [(j + ep_size // 2) % ep_size for j in range(ep_size)]
    order = [j for j in order if j != 0] + [0]
    for j in order:
        block = lax.rem(me + j, ep_size)
        for k in range(1, tp_size):
            target = lax.rem(part + k, tp_size)
            copy = remote(
                part_ref.at[block, :, columns(target)], landed.at[k, block],
                p_send.at[j, k], p_recv.at[j, k], me, target,
            )
            copy.start()
            waits.append(copy)
    for k in range(1, tp_size):
        target = lax.rem(part + k, tp_size)
        copy = remote(mix.at[target], mix_landed.at[k], m_send.at[k], m_recv.at[k], me, target)
        copy.start()
        waits.append(copy)
    for j in order:
        block = lax.rem(me + j, ep_size)
        total = part_ref[block, :, columns(part)].astype(jnp.float32)
        for k in range(1, tp_size):
            here = landed.at[k, block]
            remote(here, here, p_send.at[j, k], p_recv.at[j, k], me, part).wait_recv()
            total = total + landed[k, block].astype(jnp.float32)
        if j == 0:
            comb[me] = total.astype(jnp.bfloat16)
        else:
            reduced[block] = total.astype(jnp.bfloat16)
            copy = remote(
                reduced.at[block], comb.at[me], r_send.at[j], r_recv.at[j], block, part
            )
            copy.start()
            waits.append(copy)
    total = mix[part].astype(jnp.float32)
    for k in range(1, tp_size):
        here = mix_landed.at[k]
        remote(here, here, m_send.at[k], m_recv.at[k], me, part).wait_recv()
        total = total + mix_landed[k].astype(jnp.float32)
    mixed[...] = total.astype(jnp.bfloat16)
    for j in range(1, ep_size):
        here = comb.at[lax.rem(me - j + ep_size, ep_size)]
        remote(here, here, r_send.at[j], r_recv.at[j], me, part).wait_recv()
    for copy in waits:
        copy.wait_send()


def reduce_all(part, mix):
    ep_size, tp_size = lax.axis_size("ep"), lax.axis_size("tp")
    slots, width = part.shape[1:]
    features = width // tp_size
    dma = pltpu.SemaphoreType.DMA
    return pl.pallas_call(
        functools.partial(reduce_kernel, ep_size, tp_size),
        out_shape=(
            jax.ShapeDtypeStruct((ep_size, slots, features), jnp.bfloat16),
            jax.ShapeDtypeStruct(mix.shape[1:], jnp.bfloat16),
        ),
        in_specs=vmem(2),
        out_specs=tuple(vmem(2)),
        scratch_shapes=[
            pltpu.VMEM((tp_size, ep_size, slots, features), jnp.bfloat16),
            pltpu.VMEM(mix.shape, jnp.bfloat16),
            pltpu.VMEM((ep_size, slots, features), jnp.bfloat16),
            dma((ep_size, tp_size)), dma((ep_size, tp_size)),
            dma((tp_size,)), dma((tp_size,)), dma((ep_size,)), dma((ep_size,)), dma((1,)),
        ],
        compiler_params=pltpu.CompilerParams(
            collective_id=1, has_side_effects=True, vmem_limit_bytes=60 * 1024 * 1024
        ),
    )(part, mix)


def expert_kernel(steps, index, tokens, gate_ref, up_ref, down_ref, out, rows, total):
    step = pl.program_id(0)

    @pl.when(step == 0)
    def _():
        places = lax.broadcasted_iota(jnp.int32, (rows.shape[0], tokens.shape[0]), 1)
        choice = jnp.where(index[...] == places, 1.0, 0.0).astype(jnp.bfloat16)
        rows[...] = jnp.dot(choice, tokens[...], preferred_element_type=jnp.float32).astype(
            jnp.bfloat16
        )
        total[...] = jnp.zeros_like(total)

    gate = jnp.dot(rows[...], gate_ref[...], preferred_element_type=jnp.float32)
    up = jnp.dot(rows[...], up_ref[...], preferred_element_type=jnp.float32)
    hidden = (gate / (1.0 + jnp.exp(-gate)) * up).astype(jnp.bfloat16)
    total[...] += jnp.dot(hidden, down_ref[...], preferred_element_type=jnp.float32)

    @pl.when(step == steps - 1)
    def _():
        out[...] = total[...].astype(jnp.bfloat16)


def run_expert(index, tokens, gate_weight, up_weight, down_weight):
    count, width = index.shape[0], tokens.shape[1]
    units = gate_weight.shape[1]
    block = min(256, units)
    steps = units // block
    return pl.pallas_call(
        functools.partial(expert_kernel, steps),
        grid=(steps,),
        out_shape=jax.ShapeDtypeStruct((count, width), jnp.bfloat16),
        in_specs=[
            pl.BlockSpec(memory_space=pltpu.VMEM),
            pl.BlockSpec(memory_space=pltpu.VMEM),
            pl.BlockSpec((width, block), lambda i: (0, i)),
            pl.BlockSpec((width, block), lambda i: (0, i)),
            pl.BlockSpec((block, width), lambda i: (i, 0)),
        ],
        out_specs=pl.BlockSpec((count, width), lambda i: (0, 0)),
        scratch_shapes=[
            pltpu.VMEM((count, width), jnp.bfloat16),
            pltpu.VMEM((count, width), jnp.float32),
        ],
        compiler_params=pltpu.CompilerParams(vmem_limit_bytes=60 * 1024 * 1024),
    )(index, tokens, gate_weight, up_weight, down_weight)


def rms_scale(values, gain):
    wide = values.astype(jnp.float32)
    return wide * lax.rsqrt(jnp.mean(wide * wide, -1, keepdims=True) + eps_norm) * gain


def rotate(values, cosine, sine):
    first, second = jnp.split(values, 2, axis=-1)
    return jnp.concatenate([first * cosine - second * sine, first * sine + second * cosine], -1)


def angles(positions):
    inverse = rope_base ** (-jnp.arange(0, ROPE, 2).astype(jnp.float32) / ROPE)
    phase = positions[:, None] * inverse[None, :]
    return (jnp.cos(phase), jnp.sin(phase))


def latents(kv_latent, rope_key, kv_gain):
    token_count = kv_latent.shape[0]
    offset = lax.axis_index("ep") * token_count
    positions = (offset + jnp.arange(token_count, dtype=jnp.int32)).astype(jnp.float32)
    cosine, sine = angles(positions)
    kv_normed = rms_scale(kv_latent, kv_gain).astype(jnp.bfloat16)
    key_turned = rotate(rope_key.astype(jnp.float32), cosine, sine).astype(jnp.bfloat16)
    width = kv_latent.shape[1] + rope_key.shape[1]
    spare = jnp.zeros((token_count, -width % 128), jnp.bfloat16)
    return jnp.concatenate([kv_normed, key_turned, spare], 1), cosine, sine


def queries(q_latent, q_gain, w_query, cosine, sine):
    token_count = q_latent.shape[0]
    head_count = w_query.shape[1] // (NOPE + ROPE)
    q_normed = rms_scale(q_latent, q_gain).astype(jnp.bfloat16)
    query = jnp.dot(q_normed, w_query, preferred_element_type=jnp.float32).astype(jnp.bfloat16)
    query = query.reshape(token_count, head_count, NOPE + ROPE)
    q_pass = query[:, :, :NOPE]
    q_turned = rotate(
        query[:, :, NOPE:].astype(jnp.float32), cosine[:, None, :], sine[:, None, :]
    ).astype(jnp.bfloat16)
    return q_pass, q_turned


def attend(q_pass, q_turned, latent, turned, w_key, w_value, w_mix_out):
    token_count, head_count = q_pass.shape[:2]
    factor = (NOPE + ROPE) ** (-0.5)
    count = latent.shape[0]
    keys = jnp.dot(latent, w_key, preferred_element_type=jnp.float32).astype(jnp.bfloat16)
    keys = keys.reshape(count, head_count, NOPE)
    values = jnp.dot(latent, w_value, preferred_element_type=jnp.float32).astype(jnp.bfloat16)
    values = values.reshape(count, head_count, VDIM)
    scores = jnp.einsum("qhd,khd->hqk", q_pass, keys, preferred_element_type=jnp.float32)
    scores = (
        scores + jnp.einsum("qhd,kd->hqk", q_turned, turned, preferred_element_type=jnp.float32)
    ) * factor
    peak = jnp.max(scores, -1)
    weights = jnp.exp(scores - peak[:, :, None])
    total = jnp.sum(weights, -1)
    summed = jnp.einsum(
        "hqk,khd->qhd", weights.astype(jnp.bfloat16), values, preferred_element_type=jnp.float32
    )
    attended = (summed / jnp.transpose(total)[:, :, None]).astype(jnp.bfloat16)
    attended = attended.reshape(token_count, head_count * VDIM)
    return jnp.dot(attended, w_mix_out, preferred_element_type=jnp.float32).astype(jnp.bfloat16)


def routing(routes):
    token_count, choose = routes.shape
    expert_count = lax.axis_size("ep")
    slots = 2 * choose * token_count // expert_count
    flat_expert = routes.reshape(-1)
    onehot = (flat_expert[:, None] == jnp.arange(expert_count, dtype=jnp.int32)[None, :]).astype(
        jnp.int32
    )
    before = jnp.sum((jnp.cumsum(onehot, 0) - onehot) * onehot, 1)
    target = flat_expert * slots + before
    source = jnp.arange(token_count * choose, dtype=jnp.int32) // choose
    table = jnp.zeros((expert_count * slots,), jnp.int32).at[target].set(source)
    table = table.reshape(expert_count, 1, slots)
    table = jnp.pad(table, ((0, 0), (0, 7), (0, -slots % 128)))
    return target, table, slots


def normalize(expert_in, norm_gain):
    wide = expert_in.astype(jnp.float32)
    centered = wide - jnp.mean(wide, -1, keepdims=True)
    return (
        centered
        * lax.rsqrt(jnp.mean(centered * centered, -1, keepdims=True) + eps_norm)
        * norm_gain
    ).astype(jnp.bfloat16)


def body(
    q_latent,
    kv_latent,
    rope_key,
    q_gain,
    kv_gain,
    w_query,
    w_key,
    w_value,
    w_mix_out,
    expert_in,
    norm_gain,
    routes,
    route_scores,
    w_gate,
    w_up,
    w_down,
):
    ep_size, tp_size = lax.axis_size("ep"), lax.axis_size("tp")
    token_count, width = expert_in.shape
    choose = routes.shape[1]
    target, table, slots = routing(routes)
    normed = normalize(expert_in, norm_gain)
    packed, cosine, sine = latents(kv_latent, rope_key, kv_gain)
    all_packed, all_normed, arrived_table = gather_all(
        packed.reshape(tp_size, -1, packed.shape[1]), normed.reshape(tp_size, -1, width), table
    )
    rank = kv_latent.shape[1]
    all_packed = all_packed.reshape(-1, packed.shape[1])
    latent, turned = all_packed[:, :rank], all_packed[:, rank : rank + ROPE]
    q_pass, q_turned = queries(q_latent, q_gain, w_query, cosine, sine)
    mix = attend(q_pass, q_turned, latent, turned, w_key, w_value, w_mix_out)
    index = arrived_table[:, 0, :slots] + jnp.arange(ep_size, dtype=jnp.int32)[:, None] * token_count
    part = run_expert(
        index.reshape(-1, 1), all_normed.reshape(-1, width), w_gate[0], w_up[0], w_down[0]
    )
    comb, mixed = reduce_all(
        part.reshape(ep_size, slots, width), mix.reshape(tp_size, -1, mix.shape[1])
    )
    shares = route_scores / jnp.sum(route_scores, -1, keepdims=True)
    picked = jnp.take(comb.reshape(ep_size * slots, -1), target, axis=0, mode="clip")
    picked = picked.reshape(token_count, choose, -1).astype(jnp.float32)
    expert_out = jnp.sum(picked * shares[:, :, None], 1).astype(jnp.bfloat16)
    return (mixed, expert_out)


def solution(mesh):
    in_specs = (
        P("ep", None),
        P("ep", None),
        P("ep", None),
        P(),
        P(),
        P(None, "tp"),
        P(None, "tp"),
        P(None, "tp"),
        P("tp", None),
        P("ep", None),
        P(),
        P("ep", None),
        P("ep", None),
        P("ep", None, "tp"),
        P("ep", None, "tp"),
        P("ep", "tp", None),
    )
    out_specs = (P(("ep", "tp"), None), P("ep", "tp"))
    return jax.shard_map(body, mesh=mesh, in_specs=in_specs, out_specs=out_specs, check_vma=False)
```

profile of v0, /device:TPU:0, one launch (start us, length us, event | category | flops | bytes accessed | tf_op | source)
XLA Modules:
  0.0 129.7 jit_solution(16890696788889807591)
XLA Ops:
  0.6 0.0 copy-start
  0.6 0.0 copy-start.2
  0.7 0.0 copy-start.9
  0.7 0.9 convert_element_type.76
  1.6 0.2 multiply_cosine_fusion
  1.8 0.1 copy.41
  1.9 0.1 copy.40
  2.1 1.0 fusion.29
  3.1 1.0 fusion.31
  4.1 0.1 pad.10.clone
  4.2 0.8 maximum_maximum_fusion
  4.9 1.2 convert_reduce_fusion
  6.1 1.3 %fusion.20 = f32[128]{0:T(128)S(1)} fusion(bf16[128,2048]{1,0:T(8,128)(2,1)} %param.25, f32[128]{0:T(128)S(1)} %broadcast_multiply_fusion.1), kind=kLoop, calls=%fused_computation.21 | loop fusion | flops 1048448 | bytes 525312 | tf_op jit(solution)/shard_map/reduce_sum | solution.py:367
  7.5 0.0 copy-done.2
  7.5 1.9 %fusion.22 = bf16[128,2048]{1,0:T(8,128)(2,1)} fusion(bf16[128,2048]{1,0:T(8,128)(2,1)S(1)} %copy-done.2, f32[2048]{0:T(1024)} %param.26, f32[128]{0:T(128)S(1)} %add_rsqrt_fusion.2, f32[128]{0:T(128)S(1)} %broadcast_multiply_fusion.1), kind=kLoop, calls=%fused_computation.23 | loop fusion | flops 1310720 | bytes 1057792 | tf_op jit(solution)/shard_map/convert_element_type | solution.py:369
  9.3 0.0 copy-done.9
  9.3 0.1 copy.42
  9.5 0.1 mul.197
  9.6 0.1 copy.43
  9.7 0.1 eq.29
  9.9 0.6 reduce-window.6
  10.4 0.2 slice_reduce_fusion
  10.7 0.1 eq.25
  10.9 0.1 fusion.42
  11.0 1.4 %scatter_custom_fusion = s32[512]{0:T(512)S(1)} fusion(s32[256]{0:T(256)S(1)} %bitcast.68, s32[256]{0:T(256)S(1)} %and_select_fusion, s32[]{:T(128)} %constant.56.clone.1), kind=kCustom, calls=%fused_computation.69 | custom fusion | bytes 2052 | tf_op jit(solution)/shard_map/scatter | solution.py:356
  12.4 0.1 reshape.220
  12.5 0.6 pad.4.tab
  13.1 38.6 %shard_map.167 = (bf16[8,4,48,384]{3,2,1,0:T(8,128)(2,1)}, bf16[8,4,32,2048]{3,2,1,0:T(8,128)(2,1)}, s32[8,8,128]{2,1,0:T(8,128)}) custom-call(bf16[4,48,384]{2,1,0:T(8,128)(2,1)} %bitcast.64, bf16[4,32,2048]{2,1,0:T(8,128)(2,1)} %bitcast.63, s32[8,8,128]{2,1,0:T(8,128)} %pad.4.tab), custom_call_target="tpu_custom_call" | custom-call | tf_op jit(solution)/shard_map/pallas_call | solution.py:128
  51.7 0.8 slice_reduce_fusion.1
  52.5 0.1 squeeze.12
  52.5 0.1 add.102
  52.6 0.1 add.103
  52.7 0.9 copy.45.index
  53.6 15.1 %shard_map.168 = bf16[512,2048]{1,0:T(8,128)(2,1)} custom-call(s32[512,1]{1,0:T(8,128)} %copy.45.index, bf16[1024,2048]{1,0:T(8,128)(2,1)} %bitcast.58, bf16[2048,1024]{1,0:T(8,128)(2,1)} %bitcast.55, bf16[2048,1024]{1,0:T(8,128)(2,1)} %bitcast.56, bf16[1024,2048]{1,0:T(8,128)(2,1)} %bitcast.57), custom_call_target="tpu_custom_call" | custom-call | tf_op jit(solution)/shard_map/pallas_call | solution.py:261
  68.7 0.0 copy-done.3
  68.7 0.0 copy-done.6
  68.7 1.8 %convolution_convert_fusion.1 = bf16[1536,512]{0,1:T(8,128)(2,1)} fusion(bf16[256,512]{1,0:T(8,128)(2,1)S(1)} %copy-done.6, bf16[1536,384]{1,0:T(8,128)(2,1)S(1)} %bitcast.59), kind=kOutput, calls=%fused_computation.8 | convolution fusion | flops 403439616 | bytes 2621440 | tf_op jit(solution)/shard_map/dot_general | solution.py:328
  70.5 0.0 copy-done.5
  70.5 0.1 fusion.25
  70.6 0.0 copy-done.4
  70.6 0.0 copy-done.11
  70.6 1.1 convolution_convert_fusion.3
  71.7 2.1 %reshape.225 = bf16[192,4,192]{2,1,0:T(4,128)(2,1)} reshape(bf16[192,768]{1,0:T(8,128)(2,1)} %convolution_convert_fusion.3) | data formatting | bytes 589824 | tf_op jit(solution)/shard_map/reshape | solution.py:314
  73.8 1.0 slice.34
  74.8 0.8 copy.57
  75.6 0.9 convert_element_type.88
  76.6 0.0 copy-start.7
  76.6 0.8 fusion.28
  77.4 0.1 copy-done.7
  77.5 0.6 convolution_convert_fusion
  78.1 0.3 slice-done
  78.4 0.9 fusion.47
  79.3 0.8 fusion.1
  80.1 0.6 copy-done.1
  80.7 0.9 fusion.17
  81.6 0.0 copy-done
  81.6 1.5 %convolution_convert_fusion.2 = bf16[192,2048]{1,0:T(8,128)(2,1)} fusion(bf16[512,2048]{1,0:T(8,128)(2,1)S(1)} %copy-done, bf16[4,24,8,128]{3,2,1,0:T(8,128)(2,1)S(1)} %fusion.17), kind=kOutput, calls=%fused_computation.9 | convolution fusion | flops 403046400 | bytes 3080192 | tf_op jit(solution)/shard_map/dot_general | solution.py:342
  83.1 41.7 %shard_map.169 = (bf16[8,64,512]{2,1,0:T(8,128)(2,1)}, bf16[48,2048]{1,0:T(8,128)(2,1)}) custom-call(bf16[8,64,2048]{2,1,0:T(8,128)(2,1)} %bitcast.51, bf16[4,48,2048]{2,1,0:T(8,128)(2,1)} %bitcast.62), custom_call_target="tpu_custom_call" | custom-call | tf_op jit(solution)/shard_map/pallas_call | solution.py:213
  124.8 2.4 %gather_fusion = bf16[256,512]{1,0:T(8,128)(2,1)S(1)} fusion(bf16[512,512]{1,0:T(8,128)(2,1)} %bitcast.52, s32[1024]{0:T(1024)S(1)} %pad_clamp_fusion), kind=kCustom, calls=%fused_computation | custom fusion | bytes 525312 | tf_op jit(solution)/shard_map/jit(_take)/gather | solution.py:412
  127.1 0.3 reshape.230
  127.5 0.0 copy-done.10
  127.5 0.1 copy.52
  127.6 1.4 %multiply_reduce_fusion = bf16[128,512]{1,0:T(8,128)(2,1)} fusion(f32[128,2,512]{2,1,0:T(2,128)S(1)} %reshape.230, f32[128,2]{1,0:T(8,128)S(1)} %copy.52), kind=kLoop, calls=%fused_computation.26 | loop fusion | flops 196608 | bytes 656384 | tf_op jit(solution)/shard_map/reduce_sum | solution.py:414
  129.0 0.7 copy.68
  (29 shorter events, 0.2 us)
Async XLA Ops:
  0.6 81.0 %copy-start = (bf16[512,2048]{1,0:T(8,128)(2,1)S(1)}, bf16[512,2048]{1,0:T(8,128)(2,1)}, u32[]{:S(2)}) copy-start(bf16[512,2048]{1,0:T(8,128)(2,1)} %param.24) | copy-start | bytes 6291460
  0.6 6.8 %copy-start.2 = (bf16[128,2048]{1,0:T(8,128)(2,1)S(1)}, bf16[128,2048]{1,0:T(8,128)(2,1)}, u32[]{:S(2)}) copy-start(bf16[128,2048]{1,0:T(8,128)(2,1)} %param.25) | copy-start | bytes 1572868
  0.7 8.7 %copy-start.9 = (s32[128,2]{0,1:T(2,128)S(1)}, s32[128,2]{0,1:T(2,128)}, u32[]{:S(2)}) copy-start(s32[128,2]{0,1:T(2,128)} %param.27) | copy-start | bytes 3076
  53.6 15.1 %copy-start.3 = (bf16[8,4,48,384]{3,2,1,0:T(8,128)(2,1)S(1)}, bf16[8,4,48,384]{3,2,1,0:T(8,128)(2,1)}, u32[]{:S(2)}) copy-start(bf16[8,4,48,384]{3,2,1,0:T(8,128)(2,1)} %get-tuple-element.9) | copy-start | bytes 3538948
  53.6 15.1 %copy-start.6 = (bf16[256,512]{1,0:T(8,128)(2,1)S(1)}, bf16[256,512]{1,0:T(8,128)(2,1)}, u32[]{:S(2)}) copy-start(bf16[256,512]{1,0:T(8,128)(2,1)} %param.23) | copy-start | bytes 786436
  68.6 1.8 %copy-start.5 = (bf16[192,512]{1,0:T(8,128)(2,1)S(1)}, bf16[192,512]{1,0:T(8,128)(2,1)}, u32[]{:S(2)}) copy-start(bf16[192,512]{1,0:T(8,128)(2,1)} %param.16) | copy-start | bytes 589828
  68.6 1.9 %copy-start.4 = (bf16[512,768]{1,0:T(8,128)(2,1)S(1)}, bf16[512,768]{1,0:T(8,128)(2,1)}, u32[]{:S(2)}) copy-start(bf16[512,768]{1,0:T(8,128)(2,1)} %param.21) | copy-start | bytes 2359300
  68.7 2.0 %copy-start.11 = (f32[512]{0:T(512)S(1)}, f32[512]{0:T(512)}, u32[]{:S(2)}) copy-start(f32[512]{0:T(512)} %param.19) | copy-start | bytes 6148
  76.6 1.0 copy-start.7
  77.5 0.9 slice-start
  79.3 1.4 %copy-start.1 = (bf16[1536,512]{0,1:T(8,128)(2,1)S(1)}, bf16[1536,512]{0,1:T(8,128)(2,1)}, u32[]{:S(2)}) copy-start(bf16[1536,512]{0,1:T(8,128)(2,1)} %convolution_convert_fusion.1) | copy-start | bytes 4718596
  83.1 44.4 %copy-start.10 = (f32[128,2]{0,1:T(2,128)S(1)}, f32[128,2]{0,1:T(2,128)}, u32[]{:S(2)}) copy-start(f32[128,2]{0,1:T(2,128)} %param.28) | copy-start | bytes 3076
  124.7 4.3 %copy-start.8 = (bf16[48,2048]{1,0:T(8,128)(2,1)S(1)}, bf16[48,2048]{1,0:T(8,128)(2,1)}, u32[]{:S(2)}) copy-start(bf16[48,2048]{1,0:T(8,128)(2,1)} %get-tuple-element.26) | copy-start | bytes 589828
where the time goes:
time: 130 us
  Pallas kernels  95.4 us (73%)
  local copies, waits for them, and re-layouts  13.6 us (10%)
  other arithmetic  12.3 us (9%)
  matrix products  7.51 us (6%)
    pallas_call x1, Pallas kernels, reduce_all(): pl.pallas_call(functools.partial(reduce_kernel, ep_size, tp_size), out_sh...  41.7 us
    pallas_call x1, Pallas kernels, gather_all(): pl.pallas_call(functools.partial(gather_kernel, ep_size, tp_size), out_sh...  38.6 us
    pallas_call x1, Pallas kernels, run_expert(): pl.pallas_call(functools.partial(expert_kernel, steps), grid=(steps,), ou...  15.1 us

commit v1 on v0

v1 whole, which is shorter than its diff:
```python
import functools

import jax
import jax.numpy as jnp
from jax import lax
from jax.experimental import pallas as pl
from jax.experimental.pallas import tpu as pltpu
from jax.sharding import PartitionSpec as P

NOPE = 128
ROPE = 64
VDIM = 128

eps_norm = 1e-05
rope_base = 10000.0

MESH = pl.DeviceIdType.MESH
F32 = jnp.float32
BF16 = jnp.bfloat16


def remote(src, dst, send, recv, ep, tp):
    return pltpu.make_async_remote_copy(
        src_ref=src, dst_ref=dst, send_sem=send, recv_sem=recv, device_id=(ep, tp), device_id_type=MESH
    )


def dot(left, right):
    return jnp.dot(left, right, preferred_element_type=F32)


def rms_scale(values, gain):
    wide = values.astype(F32)
    return wide * lax.rsqrt(jnp.mean(wide * wide, -1, keepdims=True) + eps_norm) * gain


def rotate(values, table, copies):
    source = lax.broadcasted_iota(jnp.int32, (ROPE, 256), 0)
    lane = lax.broadcasted_iota(jnp.int32, (ROPE, 256), 1)
    same = (lane < ROPE) & (lane == source)
    turned = (lane >= 128) & (lane < 128 + ROPE) & (source == (lane - 128 + ROPE // 2) % ROPE)
    spread = jnp.where(same | turned, 1.0, 0.0).astype(BF16)
    wide = dot(values, spread)
    cosine, sine = table[:, :128], table[:, 128:]
    if copies > 1:
        cosine = jnp.concatenate([cosine] * copies, 0)
        sine = jnp.concatenate([sine] * copies, 0)
    return (wide[:, :128] * cosine + wide[:, 128:] * sine).astype(BF16)


def layer_kernel(
    sizes,
    q_lat, kv_lat, rope_key, q_gain, kv_gain, table, table_q, expert_in, norm_gain, routes, scores,
    w_query, w_key, w_value, w_mix, w_gate, w_up, w_down,
    mixed, expert_out,
    v_query, v_key, v_value, v_mix, v_gate, v_up, v_down,
    latent, kcat, vals, qcat, attended, mix_part, mix_landed,
    normed, place, facts, send_rows, twin_rows, rows, hidden, part_rows, landed, reduced, comb,
    w_sem, kz_send, kz_recv, kt_send, kt_recv, kc_send, kc_recv, ko_send, ko_recv,
    dz_send, dz_recv, dt_send, dt_recv, do_send, do_recv,
    p_send, p_recv, r_send, r_recv, m_send, m_recv,
):
    ep_size, tp_size, slots, choose, heads, split = sizes
    levels = ep_size // 2
    me = lax.axis_index("ep")
    part = lax.axis_index("tp")
    level, core = me // 2, me % 2
    twin = level * 2 + 1 - core
    tokens, width = expert_in.shape
    features = width // tp_size
    rank = kv_lat.shape[1]
    queries = q_lat.shape[0]
    waits = []

    def peer(k):
        return lax.rem(part + k, tp_size)

    def columns(index):
        return pl.ds(pl.multiple_of(index * features, features), features)

    def start(copy):
        copy.start()
        waits.append(copy)

    barrier = pltpu.get_barrier_semaphore()
    for d in range(1, ep_size):
        pl.semaphore_signal(
            barrier, inc=1, device_id=(lax.rem(me + d, ep_size), part), device_id_type=MESH
        )
    for k in range(1, tp_size):
        pl.semaphore_signal(barrier, inc=1, device_id=(me, peer(k)), device_id_type=MESH)
    loads = [
        pltpu.make_async_copy(src, dst, w_sem.at[i])
        for i, (src, dst) in enumerate((
            (w_query, v_query), (w_key, v_key), (w_value, v_value), (w_gate, v_gate),
            (w_up, v_up), (w_down, v_down), (w_mix, v_mix),
        ))
    ]
    for load in loads:
        load.start()

    kv_normed = rms_scale(kv_lat[...], kv_gain[...]).astype(BF16)
    key_turned = rotate(rope_key[...], table[...], 1)
    packed = jnp.concatenate([kv_normed, key_turned], 1)
    latent[me] = packed.reshape(latent.shape[1:])

    named = routes[...]
    experts = max(8, ep_size)
    expert = lax.broadcasted_iota(jnp.int32, (experts, tokens), 0)
    member = [expert == named[k : k + 1, :] for k in range(choose)]
    any_member = member[0]
    for k in range(1, choose):
        any_member = any_member | member[k]
    earlier = lax.broadcasted_iota(jnp.int32, (tokens, tokens), 0) < lax.broadcasted_iota(
        jnp.int32, (tokens, tokens), 1
    )
    before = dot(
        jnp.where(any_member, 1.0, 0.0).astype(BF16), jnp.where(earlier, 1.0, 0.0).astype(BF16)
    )
    spot = before + (expert * slots).astype(F32)
    targets = [
        jnp.sum(jnp.where(member[k], spot, 0.0), 0, keepdims=True) for k in range(choose)
    ]
    score = scores[...]
    shares = score / jnp.sum(score, 0, keepdims=True)
    known = jnp.concatenate(targets + [shares], 0)
    known = jnp.concatenate([known, jnp.zeros((128 - 2 * choose, tokens), F32)], 0)
    facts[...] = jnp.transpose(known)
    seat = lax.broadcasted_iota(jnp.int32, (ep_size * slots, tokens), 0).astype(F32)
    chosen = seat == targets[0]
    for k in range(1, choose):
        chosen = chosen | (seat == targets[k])
    place[...] = jnp.where(chosen, 1.0, 0.0).astype(BF16)

    wide = expert_in[...].astype(F32)
    centered = wide - jnp.mean(wide, -1, keepdims=True)
    normed[...] = (
        centered
        * lax.rsqrt(jnp.mean(centered * centered, -1, keepdims=True) + eps_norm)
        * norm_gain[...]
    ).astype(BF16)

    def seats(index):
        return place[pl.ds(pl.multiple_of(index * slots, slots), slots), :]

    send_rows[...] = dot(place[...], normed[:, columns(part)]).astype(BF16).reshape(send_rows.shape)
    twin_rows[...] = dot(seats(twin), normed[...]).astype(BF16)
    rows[me] = dot(seats(me), normed[...]).astype(BF16)

    pl.semaphore_wait(barrier, ep_size + tp_size - 2)

    chunk = part if split > 1 else 0
    for d in range(1, levels):
        target = lax.rem(level + d, levels) * 2 + core
        start(remote(
            latent.at[me, chunk], latent.at[me, chunk], kz_send.at[d], kz_recv.at[d], target, part
        ))
    start(remote(latent.at[me], latent.at[me], ko_send.at[0], ko_recv.at[0], twin, part))
    start(remote(twin_rows, rows.at[me], do_send.at[0], do_recv.at[0], twin, part))
    for d in range(1, levels):
        for c in range(2):
            target = lax.rem(level + d, levels) * 2 + c
            start(remote(
                send_rows.at[target], rows.at[me, :, columns(part)],
                dz_send.at[d, c], dz_recv.at[d, core], target, part,
            ))

    def behind(d, c):
        return lax.rem(level - d + levels, levels) * 2 + c

    loads[0].wait()
    q_normed = rms_scale(q_lat[...], q_gain[...]).astype(BF16)
    query = dot(q_normed, v_query[...])
    for h in range(heads):
        base = h * (NOPE + ROPE)
        qcat[h, :, :NOPE] = query[:, base : base + NOPE].astype(BF16)
        turn = query[:, base + NOPE : base + NOPE + ROPE].astype(BF16)
        qcat[h, :, NOPE:] = rotate(turn, table_q[...], 1)

    def pass_latents(d):
        here = latent.at[behind(d, core), chunk]
        remote(here, here, kz_send.at[d], kz_recv.at[d], twin, part).wait_recv()
        if split > 1:
            for k in range(1, tp_size):
                start(remote(here, here, kt_send.at[d, k], kt_recv.at[d, k], me, peer(k)))
        start(remote(here, here, kc_send.at[d, 0], kc_recv.at[d, 0], twin, part))

    def pass_latents_on(d):
        if split > 1:
            for k in range(1, tp_size):
                here = latent.at[behind(d, core), peer(tp_size - k)]
                remote(here, here, kt_send.at[d, k], kt_recv.at[d, k], twin, part).wait_recv()
                start(remote(here, here, kc_send.at[d, k], kc_recv.at[d, k], twin, part))

    def wait_latents(d):
        for k in range(tp_size if split > 1 else 1):
            index = peer(tp_size - k) if split > 1 else 0
            here = latent.at[behind(d, 1 - core), index]
            remote(here, here, kc_send.at[d, k], kc_recv.at[d, k], twin, part).wait_recv()

    def pass_rows(d):
        for c in range(2):
            here = rows.at[behind(d, c), :, columns(part)]
            remote(here, here, dz_send.at[d, c], dz_recv.at[d, c], twin, part).wait_recv()
            for k in range(1, tp_size):
                start(remote(here, here, dt_send.at[d, c, k], dt_recv.at[d, c, k], me, peer(k)))

    def wait_rows(d):
        if d == 0:
            here = rows.at[twin]
            remote(here, here, do_send.at[0], do_recv.at[0], twin, part).wait_recv()
            return
        for c in range(2):
            for k in range(1, tp_size):
                here = rows.at[behind(d, c), :, columns(peer(tp_size - k))]
                remote(here, here, dt_send.at[d, c, k], dt_recv.at[d, c, k], twin, part).wait_recv()

    block = min(256, v_gate.shape[1])

    def run_expert(d):
        first = lax.rem(level - d + levels, levels) * 2
        wait_rows(d)
        arrived = rows[pl.ds(first, 2)].reshape(2 * slots, width)
        for j in range(v_gate.shape[1] // block):
            units = slice(j * block, (j + 1) * block)
            gate = dot(arrived, v_gate[:, units])
            up = dot(arrived, v_up[:, units])
            hidden[:, units] = (gate / (1.0 + jnp.exp(-gate)) * up).astype(BF16)
        for n in range(tp_size):
            result = dot(hidden[...], v_down[:, n * features : (n + 1) * features]).astype(BF16)
            part_rows[pl.ds(first, 2), n] = result.reshape(2, slots, features)
        for c in range(2):
            for k in range(1, tp_size):
                start(remote(
                    part_rows.at[first + c, peer(k)], landed.at[first + c, k],
                    p_send.at[d, c, k], p_recv.at[d, c, k], me, peer(k),
                ))

    def sum_rows(d):
        for c in range(2):
            source = behind(d, c)
            total = part_rows[source, part].astype(F32)
            for k in range(1, tp_size):
                here = landed.at[source, k]
                remote(here, here, p_send.at[d, c, k], p_recv.at[d, c, k], twin, part).wait_recv()
                total = total + landed[source, k].astype(F32)
            reduced[source] = total.astype(BF16)
            if d > 0:
                start(remote(
                    reduced.at[source], comb.at[me], r_send.at[d, c], r_recv.at[d, core], source, part
                ))
        if d == 0:
            comb[me] = reduced[me]
            start(remote(
                reduced.at[twin], comb.at[me], r_send.at[0, 0], r_recv.at[0, 0], twin, part
            ))

    order = [d for d in range(1, levels)]
    for d in order:
        pass_latents(d)
    for load in loads[3:6]:
        load.wait()
    run_expert(0)
    pending = list(order)
    if pending:
        pass_rows(pending.pop(0))
    for d in order:
        pass_latents_on(d)
    here = latent.at[twin]
    remote(here, here, ko_send.at[0], ko_recv.at[0], twin, part).wait_recv()
    for d in order:
        wait_latents(d)
    for load in loads[1:3]:
        load.wait()

    length = latent.shape[0] * latent.shape[1] * latent.shape[2]
    every = latent[...].reshape(length, latent.shape[3])
    keys = dot(every[:, :rank], v_key[...]).astype(BF16)
    vals[...] = dot(every[:, :rank], v_value[...]).astype(BF16)
    for h in range(heads):
        kcat[h, :, :NOPE] = keys[:, h * NOPE : (h + 1) * NOPE]
        kcat[h, :, NOPE:] = every[:, rank : rank + 128]
    factor = (NOPE + ROPE) ** (-0.5)
    for h in range(heads):
        if pending:
            pass_rows(pending.pop(0))
        score = lax.dot_general(
            qcat[h], kcat[h], (((1,), (1,)), ((), ())), preferred_element_type=F32
        ) * factor
        peak = jnp.max(score, -1, keepdims=True)
        weights = jnp.exp(score - peak)
        total = jnp.sum(weights, -1, keepdims=True)
        summed = dot(weights.astype(BF16), vals[:, h * VDIM : (h + 1) * VDIM])
        attended[:, h * VDIM : (h + 1) * VDIM] = (summed / total).astype(BF16)
    while pending:
        pass_rows(pending.pop(0))
    loads[6].wait()
    mix_part[...] = dot(attended[...], v_mix[...]).astype(BF16).reshape(mix_part.shape)
    for k in range(1, tp_size):
        start(remote(
            mix_part.at[peer(k)], mix_landed.at[k], m_send.at[k], m_recv.at[k], me, peer(k)
        ))

    for i, d in enumerate(order):
        run_expert(d)
        sum_rows(([0] + order)[i])

    total = mix_part[part].astype(F32)
    for k in range(1, tp_size):
        here = mix_landed.at[k]
        remote(here, here, m_send.at[k], m_recv.at[k], twin, part).wait_recv()
        total = total + mix_landed[k].astype(F32)
    mixed[...] = total.astype(BF16)

    sum_rows(([0] + order)[-1])
    here = comb.at[twin]
    remote(here, here, r_send.at[0, 0], r_recv.at[0, 0], twin, part).wait_recv()
    for d in order:
        for c in range(2):
            here = comb.at[lax.rem(level + d, levels) * 2 + c]
            remote(here, here, r_send.at[d, c], r_recv.at[d, c], twin, part).wait_recv()
    back = comb[...].reshape(ep_size * slots, features)
    seat = lax.broadcasted_iota(jnp.int32, (tokens, ep_size * slots), 1).astype(F32)
    result = jnp.zeros((tokens, features), F32)
    for k in range(choose):
        pick = jnp.where(seat == facts[:, k : k + 1], 1.0, 0.0).astype(BF16)
        result = result + dot(pick, back) * facts[:, choose + k : choose + k + 1]
    expert_out[...] = result.astype(BF16)
    for copy in waits:
        copy.wait_send()


def body(
    q_latent,
    kv_latent,
    rope_key,
    q_gain,
    kv_gain,
    w_query,
    w_key,
    w_value,
    w_mix_out,
    expert_in,
    norm_gain,
    routes,
    route_scores,
    w_gate,
    w_up,
    w_down,
):
    ep_size, tp_size = lax.axis_size("ep"), lax.axis_size("tp")
    levels = ep_size // 2
    tokens, width = expert_in.shape
    count = kv_latent.shape[0]
    choose = routes.shape[1]
    slots = 2 * choose * tokens // ep_size
    heads = w_query.shape[1] // (NOPE + ROPE)
    features = width // tp_size
    units = w_gate.shape[2]
    mine = count // tp_size
    padded = -(-mine // 16) * 16
    split = tp_size if padded == mine else 1
    queries = padded * tp_size

    positions = (lax.axis_index("ep") * count + jnp.arange(count, dtype=jnp.int32)).astype(F32)
    inverse = rope_base ** (-jnp.arange(0, ROPE, 2).astype(F32) / ROPE)
    phase = positions[:, None] * inverse[None, :]
    cosine, sine = jnp.cos(phase), jnp.sin(phase)
    table = jnp.concatenate([cosine] * 4 + [-sine, sine] * 2, 1)

    def pad_rows(values):
        if padded == mine:
            return values
        values = values.reshape(tp_size, mine, values.shape[1])
        return jnp.pad(values, ((0, 0), (0, padded - mine), (0, 0))).reshape(queries, -1)

    dma = pltpu.SemaphoreType.DMA
    vmem = pl.BlockSpec(memory_space=pltpu.VMEM)
    far = pl.BlockSpec(memory_space=pl.ANY)
    wide = latent_width = kv_latent.shape[1] + 128
    chunk = count // split
    mixed, expert_out = pl.pallas_call(
        functools.partial(layer_kernel, (ep_size, tp_size, slots, choose, heads, split)),
        out_shape=(
            jax.ShapeDtypeStruct((padded, width), BF16),
            jax.ShapeDtypeStruct((tokens, features), BF16),
        ),
        in_specs=[vmem] * 11 + [far] * 7,
        out_specs=(vmem, vmem),
        scratch_shapes=[
            pltpu.VMEM(w_query.shape, BF16),
            pltpu.VMEM(w_key.shape, BF16),
            pltpu.VMEM(w_value.shape, BF16),
            pltpu.VMEM(w_mix_out.shape, BF16),
            pltpu.VMEM((width, units), BF16),
            pltpu.VMEM((width, units), BF16),
            pltpu.VMEM((units, width), BF16),
            pltpu.VMEM((ep_size, split, chunk, latent_width), BF16),
            pltpu.VMEM((heads, ep_size * count, NOPE + 128), BF16),
            pltpu.VMEM((ep_size * count, heads * VDIM), BF16),
            pltpu.VMEM((heads, queries, NOPE + 128), BF16),
            pltpu.VMEM((queries, heads * VDIM), BF16),
            pltpu.VMEM((tp_size, padded, width), BF16),
            pltpu.VMEM((tp_size, padded, width), BF16),
            pltpu.VMEM((tokens, width), BF16),
            pltpu.VMEM((ep_size * slots, tokens), BF16),
            pltpu.VMEM((tokens, 128), F32),
            pltpu.VMEM((ep_size, slots, features), BF16),
            pltpu.VMEM((slots, width), BF16),
            pltpu.VMEM((ep_size, slots, width), BF16),
            pltpu.VMEM((2 * slots, units), BF16),
            pltpu.VMEM((ep_size, tp_size, slots, features), BF16),
            pltpu.VMEM((ep_size, tp_size, slots, features), BF16),
            pltpu.VMEM((ep_size, slots, features), BF16),
            pltpu.VMEM((ep_size, slots, features), BF16),
            dma((7,)),
            dma((levels,)), dma((levels,)),
            dma((levels, tp_size)), dma((levels, tp_size)),
            dma((levels, tp_size)), dma((levels, tp_size)),
            dma((1,)), dma((1,)),
            dma((levels, 2)), dma((levels, 2)),
            dma((levels, 2, tp_size)), dma((levels, 2, tp_size)),
            dma((1,)), dma((1,)),
            dma((levels, 2, tp_size)), dma((levels, 2, tp_size)),
            dma((levels, 2)), dma((levels, 2)),
            dma((tp_size,)), dma((tp_size,)),
        ],
        compiler_params=pltpu.CompilerParams(
            collective_id=0, has_side_effects=True, vmem_limit_bytes=60 * 1024 * 1024
        ),
    )(
        pad_rows(q_latent), kv_latent, rope_key, q_gain[None, :], kv_gain[None, :], table,
        pad_rows(table), expert_in, norm_gain[None, :], routes.T, route_scores.T,
        w_query, w_key, w_value, w_mix_out, w_gate[0], w_up[0], w_down[0],
    )
    return (mixed[:mine], expert_out)


def solution(mesh):
    in_specs = (
        P("ep", None),
        P("ep", None),
        P("ep", None),
        P(),
        P(),
        P(None, "tp"),
        P(None, "tp"),
        P(None, "tp"),
        P("tp", None),
        P("ep", None),
        P(),
        P("ep", None),
        P("ep", None),
        P("ep", None, "tp"),
        P("ep", None, "tp"),
        P("ep", "tp", None),
    )
    out_specs = (P(("ep", "tp"), None), P("ep", "tp"))
    return jax.shard_map(body, mesh=mesh, in_specs=in_specs, out_specs=out_specs, check_vma=False)
```

time: 130 us -> 79.4 us (0.61)
  Pallas kernels: 95.4 us -> 71.3 us
  other arithmetic: 12.3 us -> 0.43 us
  local copies, waits for them, and re-layouts: 13.6 us -> 5.57 us
  matrix products: 7.51 us -> 0 us
    pallas_call x3 -> x1, Pallas kernels: 95.4 us -> 71.3 us  [body(): pl.pallas_call(functools.partial(layer_kernel, (ep_size, tp_size, slots,...]
    dot_general x7 -> x0, matrix products: 7.51 us -> none  [the longest x1 1.78 us: attend(): jnp.dot(latent, w_value, preferred_element_type=jnp.float32)]
    reduce_sum x8 -> x0, other arithmetic: 5.92 us -> none  [the longest x1 1.37 us: body(): expert_out = jnp.sum(picked * shares[:, :, None], 1).astype(jnp.bfloat16)]
    convert_element_type x6 -> x1, other arithmetic: 4.7 us -> 0.01 us  [body(): (lax.axis_index('ep') * count + jnp.arange(count, dtype=jnp.int32)).astyp...]
    gather x1 -> x0, local copies, waits for them, and re-layouts: 2.36 us -> none  [body(): jnp.take(comb.reshape(ep_size * slots, -1), target, axis=0, mode='clip')]
    slice x5 -> x0, local copies, waits for them, and re-layouts: 2.28 us -> none  [the longest x1 1 us: queries(): query[:, :, NOPE:].astype(jnp.float32)]
    unnamed x27 -> x3, local copies, waits for them, and re-layouts: 2.39 us -> 4.67 us
    reshape x2 -> x0, local copies, waits for them, and re-layouts: 2.16 us -> none  [the longest x1 2.08 us: queries(): query = query.reshape(token_count, head_count, NOPE + ROPE)]
where the time goes in v1:
time: 79.4 us; the launch traced here: 77.9 us
  Pallas kernels  71.3 us (90%)
  local copies, waits for them, and re-layouts  5.57 us (7%)
    pallas_call x1, Pallas kernels, body(): pl.pallas_call(functools.partial(layer_kernel, (ep_size, tp_size, slots,...  71.3 us
    unnamed x3, local copies, waits for them, and re-layouts  4.67 us

profile of v1, /device:TPU:0, one launch (start us, length us, event | category | flops | bytes accessed | tf_op | source)
XLA Modules:
  0.0 77.9 jit_solution(17946271825307320701)
XLA Ops:
  0.7 1.5 %copy.20.rope_key = bf16[192,64]{1,0:T(8,128)(2,1)} copy(bf16[192,64]{0,1:T(8,128)(2,1)} %param.18) | data formatting | bytes 49152 | tf_op args[2]
  2.1 0.4 multiply_sine_fusion
  2.6 0.9 %concatenate.3.table.table_q = f32[192,256]{1,0:T(8,128)} concatenate(f32[192,32]{1,0:T(8,128)S(1)} %get-tuple-element.4, f32[192,32]{1,0:T(8,128)S(1)} %get-tuple-element.4, f32[192,32]{1,0:T(8,128)S(1)} %get-tuple-element.4, f32[192,32]{1,0:T(8,128)S(1)} %get-tuple-element.4, f32[192,32]{1,0:T(8,128)S(1)} %get-tuple-element.3, f32[192,32]{1,0:T(8,128)S(1)} %get-tuple-element.2, ...), dimensions={1} | concatenate | bytes 393216 | tf_op jit(solution)/shard_map/concatenate | solution.py:369
  3.5 71.3 %shard_map.167 = (bf16[48,2048]{1,0:T(8,128)(2,1)}, bf16[128,512]{1,0:T(8,128)(2,1)}) custom-call(bf16[192,512]{1,0:T(8,128)(2,1)} %q_lat.1, bf16[192,256]{1,0:T(8,128)(2,1)} %kv_lat.1, bf16[192,64]{1,0:T(8,128)(2,1)} %copy.20.rope_key, f32[1,512]{1,0:T(1,128)} %bitcast.12, f32[1,256]{1,0:T(1,128)} %bitcast.13, f32[192,256]{1,0:T(8,128)} %concatenate.3.table.table_q, ...), custom_call_target="tpu_custom_call" | custom-call | tf_op jit(solution)/shard_map/pallas_call | solution.py:382
  74.8 1.6 %copy.23 = bf16[48,2048]{1,0:T(8,128)(2,1)} copy(bf16[48,2048]{1,0:T(8,128)(2,1)} %get-tuple-element.7) | data formatting | bytes 393216
  76.4 1.6 %copy.24 = bf16[128,512]{1,0:T(8,128)(2,1)} copy(bf16[128,512]{1,0:T(8,128)(2,1)} %get-tuple-element.8) | data formatting | bytes 262144
  (2 shorter events, 0.0 us)

commit v2 on v1

v2 whole, which is shorter than its diff:
```python
import functools
import math

import jax
import jax.numpy as jnp
import numpy as np
from jax import lax
from jax.experimental import pallas as pl
from jax.experimental.pallas import tpu as pltpu
from jax.sharding import PartitionSpec as P

NOPE = 128
ROPE = 64
VDIM = 128

eps_norm = 1e-05
rope_base = 10000.0

MESH = pl.DeviceIdType.MESH
F32 = jnp.float32
BF16 = jnp.bfloat16


def remote(src, dst, send, recv, ep, tp):
    return pltpu.make_async_remote_copy(
        src_ref=src, dst_ref=dst, send_sem=send, recv_sem=recv, device_id=(ep, tp), device_id_type=MESH
    )


def dot(left, right):
    return jnp.dot(left, right, preferred_element_type=F32)


def rms_scale(values, gain):
    wide = values.astype(F32)
    return wide * lax.rsqrt(jnp.mean(wide * wide, -1, keepdims=True) + eps_norm) * gain


def rotate(values, angles, axis):
    source = lax.broadcasted_iota(jnp.int32, (ROPE, 256), 0)
    lane = lax.broadcasted_iota(jnp.int32, (ROPE, 256), 1)
    same = (lane < 128) & (source == lane % ROPE)
    turned = (lane >= 128) & (source == (lane + ROPE // 2) % ROPE)
    spread = jnp.where(same | turned, 1.0, 0.0).astype(BF16)
    wide = lax.dot_general(
        values, spread, (((axis,), (0,)), ((), ())), preferred_element_type=F32
    )
    return (wide[:, :128] * angles[0] + wide[:, 128:] * angles[1]).astype(BF16)


def layer_kernel(
    sizes,
    q_lat, kv_lat, rope_key, q_gain, kv_gain, near_angle, far_angle, expert_in, norm_gain, routes, scores,
    w_query, w_key, w_value, w_mix, w_gate, w_up, w_down,
    mixed_far, expert_far,
    mixed, expert_out, v_query, v_key, v_value, v_mix, v_gate, v_up, v_down,
    latent, turned, kcat, vals, qcat, attended, mix_part, mix_first, mix_pair, mix_second,
    normed, place, facts, send_rows, twin_rows, rows, hidden, part_rows, first_rows, pair_rows, second_rows,
    reduced, comb,
    w_sem, kz_send, kz_recv, kc_send, kc_recv, ko_send, ko_recv,
    dz_send, dz_recv, dt_send, dt_recv, do_send, do_recv,
    p_send, p_recv, q_send, q_recv, r_send, r_recv, m_send, m_recv, n_send, n_recv,
):
    ep_size, tp_size, slots, choose, heads, extent = sizes
    levels = ep_size // 2
    me = lax.axis_index("ep")
    part = lax.axis_index("tp")
    level, core = me // 2, me % 2
    twin = level * 2 + 1 - core
    spot_of = (part % extent[0], part // extent[0])
    tokens, width = expert_in.shape
    features = width // tp_size
    rank = kv_lat.shape[1]
    waits = []

    def start(copy):
        copy.start()
        waits.append(copy)

    def columns(index):
        return pl.ds(pl.multiple_of(index * features, features), features)

    def step(axis, k):
        return lax.rem(spot_of[axis] + k, extent[axis])

    def at(axis, first, second):
        return second * extent[0] + first if axis == 0 else first * extent[0] + second

    def facing(d):
        if levels & (levels - 1):
            return lax.rem(level + d, levels), lax.rem(level - d + levels, levels)
        other = level
        bit = 1
        while bit < levels:
            if d & bit:
                other = other + bit * (1 - 2 * (level // bit % 2))
            bit *= 2
        return other, other

    barrier = pltpu.get_barrier_semaphore()
    for d in range(1, ep_size):
        pl.semaphore_signal(
            barrier, inc=1, device_id=(lax.rem(me + d, ep_size), part), device_id_type=MESH
        )
    for k in range(1, tp_size):
        pl.semaphore_signal(
            barrier, inc=1, device_id=(me, lax.rem(part + k, tp_size)), device_id_type=MESH
        )
    loads = [
        pltpu.make_async_copy(src, dst, w_sem.at[i])
        for i, (src, dst) in enumerate((
            (w_query, v_query), (w_gate, v_gate), (w_up, v_up), (w_down, v_down),
            (w_key, v_key), (w_value, v_value), (w_mix, v_mix),
        ))
    ]
    loads[0].start()

    count = kv_lat.shape[0]
    block_cosine = far_angle[me][:, :128]
    block_sine = far_angle[me][:, 128:]

    def turn_by(first, last):
        own_cosine, own_sine = near_angle[first:last, :128], near_angle[first:last, 128:]
        lane = lax.broadcasted_iota(jnp.int32, own_sine.shape, 1)
        sine = block_sine * own_cosine + block_cosine * own_sine
        return (
            block_cosine * own_cosine - block_sine * own_sine,
            jnp.where(lane % ROPE < ROPE // 2, -sine, sine),
        )

    angles = turn_by(0, count)
    angles_q = angles if q_lat.shape[0] == count else turn_by(count, count + q_lat.shape[0])
    kv_normed = rms_scale(kv_lat[...], kv_gain[...]).astype(BF16)
    key_turned = rotate(rope_key[...], angles, 0)
    latent[me] = kv_normed
    low = lax.broadcasted_iota(jnp.int32, (count // 2, 128), 1) < ROPE
    turned[me] = jnp.where(low, key_turned[: count // 2], key_turned[count // 2 :])

    for load in loads[1:]:
        load.start()
    named = routes[...]
    experts = max(8, ep_size)
    expert = lax.broadcasted_iota(jnp.int32, (experts, tokens), 0)
    member = [expert == named[k : k + 1, :] for k in range(choose)]
    any_member = member[0]
    for k in range(1, choose):
        any_member = any_member | member[k]
    earlier = lax.broadcasted_iota(jnp.int32, (tokens, tokens), 0) < lax.broadcasted_iota(
        jnp.int32, (tokens, tokens), 1
    )
    before = dot(
        jnp.where(any_member, 1.0, 0.0).astype(BF16), jnp.where(earlier, 1.0, 0.0).astype(BF16)
    )
    spot = before + (expert * slots).astype(F32)
    targets = [
        jnp.sum(jnp.where(member[k], spot, 0.0), 0, keepdims=True) for k in range(choose)
    ]
    score = scores[...]
    shares = score / jnp.sum(score, 0, keepdims=True)
    known = jnp.concatenate(targets + [shares], 0)
    known = jnp.concatenate([known, jnp.zeros((128 - 2 * choose, tokens), F32)], 0)
    facts[...] = jnp.transpose(known)
    seat = lax.broadcasted_iota(jnp.int32, (ep_size * slots, tokens), 0).astype(F32)
    chosen = seat == targets[0]
    for k in range(1, choose):
        chosen = chosen | (seat == targets[k])
    place[...] = jnp.where(chosen, 1.0, 0.0).astype(BF16)

    wide = expert_in[...].astype(F32)
    centered = wide - jnp.mean(wide, -1, keepdims=True)
    normed[...] = (
        centered
        * lax.rsqrt(jnp.mean(centered * centered, -1, keepdims=True) + eps_norm)
        * norm_gain[...]
    ).astype(BF16)


    def seats(index):
        return place[pl.ds(pl.multiple_of(index * slots, slots), slots), :]

    send_rows[...] = dot(place[...], normed[:, columns(part)]).astype(BF16).reshape(send_rows.shape)
    twin_rows[...] = dot(seats(twin), normed[...]).astype(BF16)
    rows[me] = dot(seats(me), normed[...]).astype(BF16)

    pl.semaphore_wait(barrier, ep_size + tp_size - 2)

    outs = [
        pltpu.make_async_copy(mixed, mixed_far, w_sem.at[7]),
        pltpu.make_async_copy(expert_out, expert_far, w_sem.at[8]),
    ]
    near = list(range(1, levels))
    order = near[:1] + near[:0:-1]
    start(remote(twin_rows, rows.at[me], do_send.at[0], do_recv.at[0], twin, part))
    for i, whole in enumerate((latent, turned)):
        start(remote(whole.at[me], whole.at[me], ko_send.at[i], ko_recv.at[i], twin, part))

    class Share:
        def __init__(self, view, sends, recvs, axis):
            self.view, self.sends, self.recvs, self.axis = view, sends, recvs, axis
            self.first, self.second = extent[axis], extent[1 - axis]

        def number(self, k, j):
            if j == 0:
                return k - 1
            if k == 0:
                return self.first - 1 + j - 1
            return self.first + self.second - 2 + (k - 1) * (self.second - 1) + j - 1

        def index(self, k, j):
            axis = self.axis
            return at(axis, step(axis, self.first - k if k else 0), step(1 - axis, self.second - j if j else 0))

        def push(self, here, k, j, target):
            number = self.number(k, j)
            start(remote(here, here, self.sends(number), self.recvs(number), me, target))

        def arrive(self, k, j):
            number, index = self.number(k, j), self.index(k, j)
            here = self.view(index)
            remote(here, here, self.sends(number), self.recvs(number), twin, part).wait_recv()
            return here

        def direct(self):
            axis, here = self.axis, self.view(part)
            for k in range(1, self.first):
                self.push(here, k, 0, at(axis, step(axis, k), spot_of[1 - axis]))
            for j in range(1, self.second):
                self.push(here, 0, j, at(axis, spot_of[axis], step(1 - axis, j)))

        def relay(self):
            axis = self.axis
            for k in range(1, self.first):
                here = self.arrive(k, 0)
                for j in range(1, self.second):
                    self.push(here, k, j, at(axis, spot_of[axis], step(1 - axis, j)))

        def finish(self):
            for j in range(1, self.second):
                for k in range(self.first):
                    self.arrive(k, j)

    class Sum:
        def __init__(self, whole, one, pair, two, s1, r1, s2, r2, axis):
            self.whole, self.one, self.pair, self.two = whole, one, pair, two
            self.s1, self.r1, self.s2, self.r2, self.axis = s1, r1, s2, r2, axis
            self.first, self.second = extent[axis], extent[1 - axis]

        def strip(self, index):
            return self.whole.at[:, index] if self.axis == 0 else self.whole.at[index]

        def begin(self):
            axis = self.axis
            for k in range(1, self.first):
                start(remote(
                    self.strip(step(axis, k)), self.one.at[k - 1, pl.ds(0, self.second)],
                    self.s1(k - 1), self.r1(k - 1),
                    me, at(axis, step(axis, k), spot_of[1 - axis]),
                ))

        def part_sum(self, j):
            axis = self.axis
            row = step(1 - axis, j)
            mine = self.whole[row, spot_of[0]] if axis == 0 else self.whole[spot_of[1], row]
            total = mine.astype(F32)
            for k in range(1, self.first):
                total = total + self.one[k - 1, row].astype(F32)
            return total

        def middle(self):
            axis = self.axis
            for k in range(1, self.first):
                here = self.one.at[k - 1, pl.ds(0, self.second)]
                remote(here, here, self.s1(k - 1), self.r1(k - 1), twin, part).wait_recv()
            for j in range(1, self.second):
                self.pair[j - 1] = self.part_sum(j).astype(BF16)
            for j in range(1, self.second):
                start(remote(
                    self.pair.at[j - 1], self.two.at[j - 1], self.s2(j - 1), self.r2(j - 1),
                    me, at(axis, spot_of[axis], step(1 - axis, j)),
                ))

        def end(self):
            total = self.part_sum(0)
            for j in range(1, self.second):
                here = self.two.at[j - 1]
                remote(here, here, self.s2(j - 1), self.r2(j - 1), twin, part).wait_recv()
                total = total + self.two[j - 1].astype(F32)
            return total

    def latent_send(d):
        target = facing(d)[0] * 2 + core
        for i, whole in enumerate((latent, turned)):
            here = whole.at[me]
            start(remote(here, here, kz_send.at[d, i], kz_recv.at[d, i], target, part))

    def latent_pass(d):
        for i, whole in enumerate((latent, turned)):
            here = whole.at[facing(d)[1] * 2 + core]
            remote(here, here, kz_send.at[d, i], kz_recv.at[d, i], twin, part).wait_recv()
            start(remote(here, here, kc_send.at[d, i], kc_recv.at[d, i], twin, part))

    def latent_twin(d):
        for i, whole in enumerate((latent, turned)):
            if d == 0:
                here = whole.at[twin]
                remote(here, here, ko_send.at[i], ko_recv.at[i], twin, part).wait_recv()
            else:
                here = whole.at[facing(d)[1] * 2 + 1 - core]
                remote(here, here, kc_send.at[d, i], kc_recv.at[d, i], twin, part).wait_recv()

    def row_send(d, cores=(0, 1)):
        for c in cores:
            target = facing(d)[0] * 2 + c
            start(remote(
                send_rows.at[target], rows.at[me, :, columns(part)],
                dz_send.at[d, c], dz_recv.at[d, core], target, part,
            ))

    def row_share(d, c):
        block = facing(d)[1] * 2 + c
        return Share(
            lambda index: rows.at[block, :, columns(index)],
            lambda n: dt_send.at[d, c, n], lambda n: dt_recv.at[d, c, n], c,
        )

    def row_direct(d, cores=(0, 1)):
        for c in cores:
            here = rows.at[facing(d)[1] * 2 + c, :, columns(part)]
            remote(here, here, dz_send.at[d, c], dz_recv.at[d, c], twin, part).wait_recv()
            row_share(d, c).direct()

    def row_relay(d):
        for c in range(2):
            row_share(d, c).relay()

    def row_finish(d):
        if d == 0:
            here = rows.at[twin]
            remote(here, here, do_send.at[0], do_recv.at[0], twin, part).wait_recv()
            return
        for c in range(2):
            row_share(d, c).finish()

    def row_sum(d, c):
        block = facing(d)[1] * 2 + c
        return Sum(
            part_rows.at[block], first_rows.at[block], pair_rows.at[block], second_rows.at[block],
            lambda n: p_send.at[d, c, n], lambda n: p_recv.at[d, c, n],
            lambda n: q_send.at[d, c, n], lambda n: q_recv.at[d, c, n], c,
        )

    block = min(256, v_gate.shape[1])

    def run_expert(d):
        first = facing(d)[1] * 2
        arrived = rows[pl.ds(first, 2)].reshape(2 * slots, width)
        for j in range(v_gate.shape[1] // block):
            units = slice(j * block, (j + 1) * block)
            gate = dot(arrived, v_gate[:, units])
            up = dot(arrived, v_up[:, units])
            hidden[:, units] = (gate / (1.0 + jnp.exp(-gate)) * up).astype(BF16)
        for n in range(tp_size):
            result = dot(hidden[...], v_down[:, n * features : (n + 1) * features]).astype(BF16)
            part_rows[pl.ds(first, 2), n // extent[0], n % extent[0]] = result.reshape(2, slots, features)

    def sum_begin(d):
        for c in range(2):
            row_sum(d, c).begin()

    def sum_middle(d):
        for c in range(2):
            row_sum(d, c).middle()

    def sum_end(d):
        other = facing(d)[1]
        for c in range(2):
            reduced[other * 2 + c] = row_sum(d, c).end().astype(BF16)
        if d == 0:
            comb[me] = reduced[me]
            start(remote(reduced.at[twin], comb.at[me], r_send.at[0, 0], r_recv.at[0, 0], twin, part))
            return
        for c in range(2):
            source = other * 2 + c
            start(remote(
                reduced.at[source], comb.at[me], r_send.at[d, c], r_recv.at[d, core], source, part
            ))

    def mix_sum(h):
        return Sum(
            mix_part.at[h], mix_first.at[h], mix_pair.at[h], mix_second.at[h],
            lambda n: m_send.at[h, n], lambda n: m_recv.at[h, n],
            lambda n: n_send.at[h, n], lambda n: n_recv.at[h, n], h,
        )

    def queries():
        loads[0].wait()
        q_normed = rms_scale(q_lat[...], q_gain[...]).astype(BF16)
        query = dot(q_normed, v_query[...])
        for h in range(heads):
            base = h * (NOPE + ROPE)
            qcat[h, :, :NOPE] = query[:, base : base + NOPE].astype(BF16)
            turn = query[:, base + NOPE : base + NOPE + ROPE].astype(BF16)
            qcat[h, :, NOPE:] = rotate(turn, angles_q, 1)

    def make_keys(d):
        first = facing(d)[1] * 2
        span = 2 * count
        tokens_in = pl.ds(pl.multiple_of(first * count, span), span)
        some = latent[pl.ds(first, 2)].reshape(span, rank)
        keys = dot(some, v_key[...]).astype(BF16)
        vals[tokens_in, :] = dot(some, v_value[...]).astype(BF16)
        both = turned[pl.ds(first, 2)]
        low = lax.broadcasted_iota(jnp.int32, both.shape, 2) < ROPE
        none = jnp.zeros_like(both)
        spread = jnp.concatenate([jnp.where(low, both, none), jnp.where(low, none, both)], 1)
        for h in range(heads):
            kcat[h, tokens_in, :NOPE] = keys[:, h * NOPE : (h + 1) * NOPE]
            kcat[h, tokens_in, NOPE:] = spread.reshape(span, 128)

    def attend(h):
        factor = (NOPE + ROPE) ** (-0.5)
        score = lax.dot_general(
            qcat[h], kcat[h], (((1,), (1,)), ((), ())), preferred_element_type=F32
        ) * factor
        peak = jnp.max(score, -1, keepdims=True)
        weights = jnp.exp(score - peak)
        total = jnp.sum(weights, -1, keepdims=True)
        summed = dot(weights.astype(BF16), vals[:, h * VDIM : (h + 1) * VDIM])
        attended[:, h * VDIM : (h + 1) * VDIM] = (summed / total).astype(BF16)

    def make_mix():
        loads[6].wait()
        half = width // 2
        for h in range(2):
            result = dot(attended[...], v_mix[:, h * half : (h + 1) * half]).astype(BF16)
            mix_part[h] = result.reshape(mix_part.shape[1:])
        for h in range(2):
            mix_sum(h).begin()

    def mix_middle():
        for h in range(2):
            mix_sum(h).middle()

    def mix_end():
        half = width // 2
        for h in range(2):
            mixed[:, h * half : (h + 1) * half] = mix_sum(h).end().astype(BF16)
        outs[0].start()

    rest = order[1:]
    for d in order[:1]:
        row_send(d)
    queries()
    for d in rest[:1]:
        row_send(d)
    for load in loads[4:6]:
        load.wait()
    latent_twin(0)
    make_keys(0)
    for load in loads[1:4]:
        load.wait()
    row_finish(0)
    run_expert(0)
    for d in order[:1]:
        row_direct(d)
    sum_begin(0)
    for d in rest[1:]:
        row_send(d)
    for d in near:
        latent_send(d)
    for d in rest[:1]:
        row_direct(d)
    for d in order[:1]:
        row_relay(d)
    sum_middle(0)
    groups = [0] + order
    last = len(order) - 1
    for i, d in enumerate(order):
        if i == last:
            for e in near:
                latent_pass(e)
            for e in near:
                latent_twin(e)
                make_keys(e)
        row_finish(d)
        if i + 1 < last:
            row_relay(order[i + 1])
        if i + 2 <= last:
            row_direct(order[i + 2])
        run_expert(d)
        sum_begin(d)
        if i + 1 == last:
            row_relay(order[last])
        if i > 0:
            sum_middle(groups[i])
            sum_end(groups[i - 1])
    for h in range(heads):
        attend(h)
    make_mix()
    for d in order[-1:]:
        sum_middle(d)
    for d in groups[max(0, len(groups) - 2) : -1]:
        sum_end(d)
    sum_end(groups[-1])
    mix_middle()
    mix_end()

    here = comb.at[twin]
    remote(here, here, r_send.at[0, 0], r_recv.at[0, 0], twin, part).wait_recv()
    for d in order:
        for c in range(2):
            here = comb.at[facing(d)[0] * 2 + c]
            remote(here, here, r_send.at[d, c], r_recv.at[d, c], twin, part).wait_recv()
    back = comb[...].reshape(ep_size * slots, features)
    seat = lax.broadcasted_iota(jnp.int32, (tokens, ep_size * slots), 1).astype(F32)
    result = jnp.zeros((tokens, features), F32)
    for k in range(choose):
        pick = jnp.where(seat == facts[:, k : k + 1], 1.0, 0.0).astype(BF16)
        result = result + dot(pick, back) * facts[:, choose + k : choose + k + 1]
    expert_out[...] = result.astype(BF16)
    outs[1].start()
    for copy in waits:
        copy.wait_send()
    for out in outs:
        out.wait()


def hand_over(mixed_in, expert_in, mixed, expert_out):
    mixed[...] = mixed_in[: mixed.shape[0]]
    expert_out[...] = expert_in[...]


def body(
    q_latent,
    kv_latent,
    rope_key,
    q_gain,
    kv_gain,
    w_query,
    w_key,
    w_value,
    w_mix_out,
    expert_in,
    norm_gain,
    routes,
    route_scores,
    w_gate,
    w_up,
    w_down,
):
    ep_size, tp_size = lax.axis_size("ep"), lax.axis_size("tp")
    levels = ep_size // 2
    tokens, width = expert_in.shape
    count = kv_latent.shape[0]
    choose = routes.shape[1]
    slots = 2 * choose * tokens // ep_size
    heads = w_query.shape[1] // (NOPE + ROPE)
    features = width // tp_size
    units = w_gate.shape[2]
    mine = count // tp_size
    padded = -(-mine // 16) * 16
    queries = padded * tp_size
    narrow = math.isqrt(tp_size)
    while tp_size % narrow:
        narrow -= 1
    extent = (tp_size // narrow, narrow)
    most = max(extent)
    ahead = max(1, most - 1)
    wing = width // 2

    lane = np.arange(128) % (ROPE // 2)
    inverse = np.float32(rope_base) ** (-(2 * lane).astype(np.float32) / np.float32(ROPE))

    def turns(positions):
        phase = positions[:, None].astype(np.float64) * inverse[None, :].astype(np.float64)
        return np.concatenate([np.cos(phase), np.sin(phase)], 1).astype(np.float32)

    near_angle = turns(np.arange(count))
    if padded != mine:
        spread = np.pad(near_angle.reshape(tp_size, mine, 256), ((0, 0), (0, padded - mine), (0, 0)))
        near_angle = np.concatenate([near_angle, spread.reshape(queries, 256)], 0)
    far_angle = turns(np.arange(ep_size) * count)[:, None, :]

    def pad_rows(values):
        if padded == mine:
            return values
        values = values.reshape(tp_size, mine, values.shape[1])
        return jnp.pad(values, ((0, 0), (0, padded - mine), (0, 0))).reshape(queries, -1)

    dma = pltpu.SemaphoreType.DMA
    vmem = pl.BlockSpec(memory_space=pltpu.VMEM)
    far = pl.BlockSpec(memory_space=pl.ANY)
    mixed, expert_out = pl.pallas_call(
        functools.partial(layer_kernel, (ep_size, tp_size, slots, choose, heads, extent)),
        out_shape=(
            jax.ShapeDtypeStruct((padded, width), BF16),
            jax.ShapeDtypeStruct((tokens, features), BF16),
        ),
        in_specs=[vmem] * 11 + [far] * 7,
        out_specs=(far, far),
        scratch_shapes=[
            pltpu.VMEM((padded, width), BF16),
            pltpu.VMEM((tokens, features), BF16),
            pltpu.VMEM(w_query.shape, BF16),
            pltpu.VMEM(w_key.shape, BF16),
            pltpu.VMEM(w_value.shape, BF16),
            pltpu.VMEM(w_mix_out.shape, BF16),
            pltpu.VMEM((width, units), BF16),
            pltpu.VMEM((width, units), BF16),
            pltpu.VMEM((units, width), BF16),
            pltpu.VMEM((ep_size, count, kv_latent.shape[1]), BF16),
            pltpu.VMEM((ep_size, count // 2, 128), BF16),
            pltpu.VMEM((heads, ep_size * count, NOPE + 128), BF16),
            pltpu.VMEM((ep_size * count, heads * VDIM), BF16),
            pltpu.VMEM((heads, queries, NOPE + 128), BF16),
            pltpu.VMEM((queries, heads * VDIM), BF16),
            pltpu.VMEM((2, extent[1], extent[0], padded, wing), BF16),
            pltpu.VMEM((2, ahead, most, padded, wing), BF16),
            pltpu.VMEM((2, ahead, padded, wing), BF16),
            pltpu.VMEM((2, ahead, padded, wing), BF16),
            pltpu.VMEM((tokens, width), BF16),
            pltpu.VMEM((ep_size * slots, tokens), BF16),
            pltpu.VMEM((tokens, 128), F32),
            pltpu.VMEM((ep_size, slots, features), BF16),
            pltpu.VMEM((slots, width), BF16),
            pltpu.VMEM((ep_size, slots, width), BF16),
            pltpu.VMEM((2 * slots, units), BF16),
            pltpu.VMEM((ep_size, extent[1], extent[0], slots, features), BF16),
            pltpu.VMEM((ep_size, ahead, most, slots, features), BF16),
            pltpu.VMEM((ep_size, ahead, slots, features), BF16),
            pltpu.VMEM((ep_size, ahead, slots, features), BF16),
            pltpu.VMEM((ep_size, slots, features), BF16),
            pltpu.VMEM((ep_size, slots, features), BF16),
            dma((9,)),
            dma((levels, 2)), dma((levels, 2)),
            dma((levels, 2)), dma((levels, 2)),
            dma((2,)), dma((2,)),
            dma((levels, 2)), dma((levels, 2)),
            dma((levels, 2, tp_size)), dma((levels, 2, tp_size)),
            dma((1,)), dma((1,)),
            dma((levels, 2, ahead)), dma((levels, 2, ahead)),
            dma((levels, 2, ahead)), dma((levels, 2, ahead)),
            dma((levels, 2)), dma((levels, 2)),
            dma((2, ahead)), dma((2, ahead)),
            dma((2, ahead)), dma((2, ahead)),
        ],
        compiler_params=pltpu.CompilerParams(
            collective_id=0, has_side_effects=True, vmem_limit_bytes=60 * 1024 * 1024
        ),
    )(
        pad_rows(q_latent), kv_latent, rope_key.T, q_gain[None, :], kv_gain[None, :], near_angle, far_angle,
        expert_in, norm_gain[None, :], routes.T, route_scores.T,
        w_query, w_key, w_value, w_mix_out, w_gate[0], w_up[0], w_down[0],
    )
    return pl.pallas_call(
        hand_over,
        out_shape=(
            jax.ShapeDtypeStruct((mine, width), BF16),
            jax.ShapeDtypeStruct((tokens, features), BF16),
        ),
        in_specs=[vmem] * 2,
        out_specs=(vmem, vmem),
    )(mixed, expert_out)


def solution(mesh):
    in_specs = (
        P("ep", None),
        P("ep", None),
        P("ep", None),
        P(),
        P(),
        P(None, "tp"),
        P(None, "tp"),
        P(None, "tp"),
        P("tp", None),
        P("ep", None),
        P(),
        P("ep", None),
        P("ep", None),
        P("ep", None, "tp"),
        P("ep", None, "tp"),
        P("ep", "tp", None),
    )
    out_specs = (P(("ep", "tp"), None), P("ep", "tp"))
    return jax.shard_map(body, mesh=mesh, in_specs=in_specs, out_specs=out_specs, check_vma=False)
```

time: 79.4 us -> 62.3 us (0.78); the launches traced: 77.9 us -> 62.1 us
  Pallas kernels: 71.3 us -> 61.4 us
  local copies, waits for them, and re-layouts: 5.57 us -> 0 us
    pallas_call x1, Pallas kernels: 71.3 us -> 59.7 us  [body(): pl.pallas_call(functools.partial(layer_kernel, (ep_size, tp_size, slots,...]
    unnamed x3 -> x0, local copies, waits for them, and re-layouts: 4.67 us -> none
    pallas_call x0 -> x1, Pallas kernels: none -> 1.74 us  [body(): pl.pallas_call(hand_over, out_shape=(jax.ShapeDtypeStruct((mine, width),...]
    concatenate x1 -> x0, local copies, waits for them, and re-layouts: 0.9 us -> none  [body(): table = jnp.concatenate([cosine] * 4 + [-sine, sine] * 2, 1)]
where the time goes in v2:
time: 62.3 us; the launch traced here: 62.1 us
  Pallas kernels  61.4 us (99%)
  between operations  0.65 us (1%)
    pallas_call x1, Pallas kernels, body(): pl.pallas_call(functools.partial(layer_kernel, (ep_size, tp_size, slots,...  59.7 us
    pallas_call x1, Pallas kernels, body(): pl.pallas_call(hand_over, out_shape=(jax.ShapeDtypeStruct((mine, width),...  1.74 us

profile of v2, /device:TPU:0, one launch (start us, length us, event | category | flops | bytes accessed | tf_op | source)
XLA Modules:
  0.0 62.1 jit_solution(12189025693150172453)
XLA Ops:
  0.6 59.7 %shard_map.185 = (bf16[48,2048]{1,0:T(8,128)(2,1)}, bf16[128,512]{1,0:T(8,128)(2,1)}) custom-call(bf16[192,512]{1,0:T(8,128)(2,1)} %q_lat.1, bf16[192,256]{1,0:T(8,128)(2,1)} %kv_lat.1, bf16[64,192]{1,0:T(8,128)(2,1)} %bitcast.12, f32[1,512]{1,0:T(1,128)} %bitcast.14, f32[1,256]{1,0:T(1,128)} %bitcast.15, f32[192,256]{1,0:T(8,128)} %constant.4.clone.near_angle, ...), custom_call_target="tpu_custom_call" | custom-call | tf_op jit(solution)/shard_map/pallas_call | solution.py:593
  60.4 1.7 %shard_map.186 = (bf16[48,2048]{1,0:T(8,128)(2,1)}, bf16[128,512]{1,0:T(8,128)(2,1)}) custom-call(bf16[48,2048]{1,0:T(8,128)(2,1)} %get-tuple-element.4.mixed_in, bf16[128,512]{1,0:T(8,128)(2,1)} %get-tuple-element.5.expert_in), custom_call_target="tpu_custom_call" | custom-call | tf_op jit(solution)/shard_map/pallas_call | solution.py:655

commit v3 on v2

--- a/solution.py
+++ b/solution.py
@@ -50,16 +50,15 @@
 
 def layer_kernel(
     sizes,
-    q_lat, kv_lat, rope_key, q_gain, kv_gain, near_angle, far_angle, expert_in, norm_gain, routes, scores,
+    h_q_lat, h_kv_lat, h_rope_key, h_q_gain, h_kv_gain, h_near_angle, h_far_angle, h_expert_in, h_norm_gain, h_routes, h_scores,
     w_query, w_key, w_value, w_mix, w_gate, w_up, w_down,
     mixed_far, expert_far,
-    mixed, expert_out, v_query, v_key, v_value, v_mix, v_gate, v_up, v_down,
+    mixed, expert_out, q_lat, kv_lat, rope_key, q_gain, kv_gain, near_angle, far_angle, expert_in, norm_gain, routes, scores,
+    v_query, v_key, v_value, v_mix, v_gate, v_up, v_down,
     latent, turned, kcat, vals, qcat, attended, mix_part, mix_first, mix_pair, mix_second,
     normed, place, facts, send_rows, twin_rows, rows, hidden, part_rows, first_rows, pair_rows, second_rows,
     reduced, comb,
-    w_sem, kz_send, kz_recv, kc_send, kc_recv, ko_send, ko_recv,
-    dz_send, dz_recv, dt_send, dt_recv, do_send, do_recv,
-    p_send, p_recv, q_send, q_recv, r_send, r_recv, m_send, m_recv, n_send, n_recv,
+    w_sem, i_sem, pool, kz_recv, kx_recv, kc_recv, ko_recv, dz_recv, dt_recv, do_recv, p_recv, q_recv, r_recv, m_recv, n_recv,
 ):
     ep_size, tp_size, slots, choose, heads, extent = sizes
     levels = ep_size // 2
@@ -70,12 +69,20 @@
     spot_of = (part % extent[0], part // extent[0])
     tokens, width = expert_in.shape
     features = width // tp_size
-    rank = kv_lat.shape[1]
+    count, rank = kv_lat.shape
     waits = []
-
-    def start(copy):
+    spun = [None]
+
+    def start(src, dst, recv, ep, tp):
+        slot = len(waits) % pool.shape[0]
+        if len(waits) >= pool.shape[0]:
+            waits[len(waits) - pool.shape[0]].wait_send()
+        copy = remote(src, dst, pool.at[slot], recv, ep, tp)
         copy.start()
         waits.append(copy)
+
+    def landed(here, recv):
+        remote(here, here, pool.at[0], recv, twin, part).wait_recv()
 
     def columns(index):
         return pl.ds(pl.multiple_of(index * features, features), features)
@@ -97,6 +104,16 @@
             bit *= 2
         return other, other
 
+    small = [
+        pltpu.make_async_copy(src, dst, i_sem.at[i])
+        for i, (src, dst) in enumerate((
+            (h_kv_lat, kv_lat), (h_rope_key, rope_key), (h_kv_gain, kv_gain), (h_near_angle, near_angle),
+            (h_far_angle, far_angle), (h_routes, routes), (h_scores, scores), (h_expert_in, expert_in),
+            (h_norm_gain, norm_gain), (h_q_lat, q_lat), (h_q_gain, q_gain),
+        ))
+    ]
+    for load in small[5:9] + small[:5] + small[9:]:
+        load.start()
     barrier = pltpu.get_barrier_semaphore()
     for d in range(1, ep_size):
         pl.semaphore_signal(
@@ -113,31 +130,14 @@
             (w_key, v_key), (w_value, v_value), (w_mix, v_mix),
         ))
     ]
-    loads[0].start()
-
-    count = kv_lat.shape[0]
-    block_cosine = far_angle[me][:, :128]
-    block_sine = far_angle[me][:, 128:]
-
-    def turn_by(first, last):
-        own_cosine, own_sine = near_angle[first:last, :128], near_angle[first:last, 128:]
-        lane = lax.broadcasted_iota(jnp.int32, own_sine.shape, 1)
-        sine = block_sine * own_cosine + block_cosine * own_sine
-        return (
-            block_cosine * own_cosine - block_sine * own_sine,
-            jnp.where(lane % ROPE < ROPE // 2, -sine, sine),
-        )
-
-    angles = turn_by(0, count)
-    angles_q = angles if q_lat.shape[0] == count else turn_by(count, count + q_lat.shape[0])
-    kv_normed = rms_scale(kv_lat[...], kv_gain[...]).astype(BF16)
-    key_turned = rotate(rope_key[...], angles, 0)
-    latent[me] = kv_normed
-    low = lax.broadcasted_iota(jnp.int32, (count // 2, 128), 1) < ROPE
-    turned[me] = jnp.where(low, key_turned[: count // 2], key_turned[count // 2 :])
-
-    for load in loads[1:]:
-        load.start()
+    for i in (4, 5, 0, 1):
+        loads[i].start()
+
+    for load in small[5:9]:
+        load.wait()
+    for i in (2, 3, 6):
+        loads[i].start()
+
     named = routes[...]
     experts = max(8, ep_size)
     expert = lax.broadcasted_iota(jnp.int32, (experts, tokens), 0)
@@ -185,18 +185,41 @@
     pl.semaphore_wait(barrier, ep_size + tp_size - 2)
 
     outs = [
-        pltpu.make_async_copy(mixed, mixed_far, w_sem.at[7]),
-        pltpu.make_async_copy(expert_out, expert_far, w_sem.at[8]),
+        pltpu.make_async_copy(mixed, mixed_far, w_sem.at[0]),
+        pltpu.make_async_copy(expert_out, expert_far, w_sem.at[1]),
     ]
     near = list(range(1, levels))
-    order = near[:1] + near[:0:-1]
-    start(remote(twin_rows, rows.at[me], do_send.at[0], do_recv.at[0], twin, part))
-    for i, whole in enumerate((latent, turned)):
-        start(remote(whole.at[me], whole.at[me], ko_send.at[i], ko_recv.at[i], twin, part))
+    order = near[::-1]
+    start(twin_rows, rows.at[me], do_recv.at[0], twin, part)
+
+    def prepare_latents():
+        for load in small[:5]:
+            load.wait()
+        block_cosine = far_angle[me][:, :128]
+        block_sine = far_angle[me][:, 128:]
+
+        def turn_by(first, last):
+            own_cosine, own_sine = near_angle[first:last, :128], near_angle[first:last, 128:]
+            lane = lax.broadcasted_iota(jnp.int32, own_sine.shape, 1)
+            sine = block_sine * own_cosine + block_cosine * own_sine
+            return (
+                block_cosine * own_cosine - block_sine * own_sine,
+                jnp.where(lane % ROPE < ROPE // 2, -sine, sine),
+            )
+
+        angles = turn_by(0, count)
+        spun[0] = angles if q_lat.shape[0] == count else turn_by(count, count + q_lat.shape[0])
+        kv_normed = rms_scale(kv_lat[...], kv_gain[...]).astype(BF16)
+        key_turned = rotate(rope_key[...], angles, 0)
+        latent[me] = kv_normed.reshape(latent.shape[1:])
+        low = lax.broadcasted_iota(jnp.int32, (count // 2, 128), 1) < ROPE
+        turned[me] = jnp.where(low, key_turned[: count // 2], key_turned[count // 2 :])
+        for i, whole in enumerate((latent, turned)):
+            start(whole.at[me], whole.at[me], ko_recv.at[i], twin, part)
 
     class Share:
-        def __init__(self, view, sends, recvs, axis):
-            self.view, self.sends, self.recvs, self.axis = view, sends, recvs, axis
+        def __init__(self, view, recvs, axis):
+            self.view, self.recvs, self.axis = view, recvs, axis
             self.first, self.second = extent[axis], extent[1 - axis]
 
         def number(self, k, j):
@@ -212,12 +235,12 @@
 
         def push(self, here, k, j, target):
             number = self.number(k, j)
-            start(remote(here, here, self.sends(number), self.recvs(number), me, target))
+            start(here, here, self.recvs(number), me, target)
 
         def arrive(self, k, j):
             number, index = self.number(k, j), self.index(k, j)
             here = self.view(index)
-            remote(here, here, self.sends(number), self.recvs(number), twin, part).wait_recv()
+            landed(here, self.recvs(number))
             return here
 
         def direct(self):
@@ -240,9 +263,9 @@
                     self.arrive(k, j)
 
     class Sum:
-        def __init__(self, whole, one, pair, two, s1, r1, s2, r2, axis):
+        def __init__(self, whole, one, pair, two, r1, r2, axis):
             self.whole, self.one, self.pair, self.two = whole, one, pair, two
-            self.s1, self.r1, self.s2, self.r2, self.axis = s1, r1, s2, r2, axis
+            self.r1, self.r2, self.axis = r1, r2, axis
             self.first, self.second = extent[axis], extent[1 - axis]
 
         def strip(self, index):
@@ -251,11 +274,9 @@
         def begin(self):
             axis = self.axis
             for k in range(1, self.first):
-                start(remote(
-                    self.strip(step(axis, k)), self.one.at[k - 1, pl.ds(0, self.second)],
-                    self.s1(k - 1), self.r1(k - 1),
-                    me, at(axis, step(axis, k), spot_of[1 - axis]),
-                ))
+                start(
+                    self.strip(step(axis, k)), self.one.at[k - 1, pl.ds(0, self.second)], self.r1(k - 1), me, at(axis, step(axis, k), spot_of[1 - axis]),
+                )
 
         def part_sum(self, j):
             axis = self.axis
@@ -270,63 +291,83 @@
             axis = self.axis
             for k in range(1, self.first):
                 here = self.one.at[k - 1, pl.ds(0, self.second)]
-                remote(here, here, self.s1(k - 1), self.r1(k - 1), twin, part).wait_recv()
+                landed(here, self.r1(k - 1))
             for j in range(1, self.second):
                 self.pair[j - 1] = self.part_sum(j).astype(BF16)
             for j in range(1, self.second):
-                start(remote(
-                    self.pair.at[j - 1], self.two.at[j - 1], self.s2(j - 1), self.r2(j - 1),
-                    me, at(axis, spot_of[axis], step(1 - axis, j)),
-                ))
+                start(
+                    self.pair.at[j - 1], self.two.at[j - 1], self.r2(j - 1), me, at(axis, spot_of[axis], step(1 - axis, j)),
+                )
 
         def end(self):
             total = self.part_sum(0)
             for j in range(1, self.second):
                 here = self.two.at[j - 1]
-                remote(here, here, self.s2(j - 1), self.r2(j - 1), twin, part).wait_recv()
+                landed(here, self.r2(j - 1))
                 total = total + self.two[j - 1].astype(F32)
             return total
 
+    halves = all(n % 2 == 0 for n in extent)
+    parity = lax.rem(spot_of[0] + spot_of[1], 2) if halves else 0
+    taken = pl.ds(2 * parity, 2) if halves else pl.ds(0, 4)
+
+    def latent_pieces(block):
+        return (latent.at[block, taken], turned.at[block])
+
     def latent_send(d):
         target = facing(d)[0] * 2 + core
-        for i, whole in enumerate((latent, turned)):
-            here = whole.at[me]
-            start(remote(here, here, kz_send.at[d, i], kz_recv.at[d, i], target, part))
+        for i, here in enumerate(latent_pieces(me)):
+            start(here, here, kz_recv.at[d - 1, i], target, part)
 
     def latent_pass(d):
-        for i, whole in enumerate((latent, turned)):
-            here = whole.at[facing(d)[1] * 2 + core]
-            remote(here, here, kz_send.at[d, i], kz_recv.at[d, i], twin, part).wait_recv()
-            start(remote(here, here, kc_send.at[d, i], kc_recv.at[d, i], twin, part))
+        block = facing(d)[1] * 2 + core
+        for i, here in enumerate(latent_pieces(block)):
+            landed(here, kz_recv.at[d - 1, i])
+        if halves:
+            for a in range(2):
+                here = latent.at[block, 2 * parity + a]
+                target = at(a, step(a, 1), spot_of[1 - a])
+                start(here, here, kx_recv.at[d - 1, a], me, target)
+        for i, here in enumerate(latent_pieces(block)):
+            start(here, here, kc_recv.at[d - 1, i], twin, part)
+
+    def latent_rest(d):
+        if halves:
+            for a in range(2):
+                here = latent.at[facing(d)[1] * 2 + core, 2 * (1 - parity) + a]
+                landed(here, kx_recv.at[d - 1, a])
+                start(here, here, kc_recv.at[d - 1, 2 + a], twin, part)
 
     def latent_twin(d):
-        for i, whole in enumerate((latent, turned)):
-            if d == 0:
+        if d == 0:
+            for i, whole in enumerate((latent, turned)):
                 here = whole.at[twin]
-                remote(here, here, ko_send.at[i], ko_recv.at[i], twin, part).wait_recv()
-            else:
-                here = whole.at[facing(d)[1] * 2 + 1 - core]
-                remote(here, here, kc_send.at[d, i], kc_recv.at[d, i], twin, part).wait_recv()
+                landed(here, ko_recv.at[i])
+            return
+        block = facing(d)[1] * 2 + 1 - core
+        for i, here in enumerate(latent_pieces(block)):
+            landed(here, kc_recv.at[d - 1, i])
+        if halves:
+            for a in range(2):
+                here = latent.at[block, 2 * (1 - parity) + a]
+                landed(here, kc_recv.at[d - 1, 2 + a])
 
     def row_send(d, cores=(0, 1)):
         for c in cores:
             target = facing(d)[0] * 2 + c
-            start(remote(
-                send_rows.at[target], rows.at[me, :, columns(part)],
-                dz_send.at[d, c], dz_recv.at[d, core], target, part,
-            ))
+            start(send_rows.at[target], rows.at[me, :, columns(part)], dz_recv.at[d - 1, core], target, part)
 
     def row_share(d, c):
         block = facing(d)[1] * 2 + c
         return Share(
             lambda index: rows.at[block, :, columns(index)],
-            lambda n: dt_send.at[d, c, n], lambda n: dt_recv.at[d, c, n], c,
+            lambda n: dt_recv.at[d - 1, c, n], c,
         )
 
     def row_direct(d, cores=(0, 1)):
         for c in cores:
             here = rows.at[facing(d)[1] * 2 + c, :, columns(part)]
-            remote(here, here, dz_send.at[d, c], dz_recv.at[d, c], twin, part).wait_recv()
+            landed(here, dz_recv.at[d - 1, c])
             row_share(d, c).direct()
 
     def row_relay(d):
@@ -336,7 +377,7 @@
     def row_finish(d):
         if d == 0:
             here = rows.at[twin]
-            remote(here, here, do_send.at[0], do_recv.at[0], twin, part).wait_recv()
+            landed(here, do_recv.at[0])
             return
         for c in range(2):
             row_share(d, c).finish()
@@ -345,8 +386,7 @@
         block = facing(d)[1] * 2 + c
         return Sum(
             part_rows.at[block], first_rows.at[block], pair_rows.at[block], second_rows.at[block],
-            lambda n: p_send.at[d, c, n], lambda n: p_recv.at[d, c, n],
-            lambda n: q_send.at[d, c, n], lambda n: q_recv.at[d, c, n], c,
+            lambda n: p_recv.at[d, c, n], lambda n: q_recv.at[d, c, n], c,
         )
 
     block = min(256, v_gate.shape[1])
@@ -359,6 +399,8 @@
             gate = dot(arrived, v_gate[:, units])
             up = dot(arrived, v_up[:, units])
             hidden[:, units] = (gate / (1.0 + jnp.exp(-gate)) * up).astype(BF16)
+        if d == 0:
+            loads[3].wait()
         for n in range(tp_size):
             result = dot(hidden[...], v_down[:, n * features : (n + 1) * features]).astype(BF16)
             part_rows[pl.ds(first, 2), n // extent[0], n % extent[0]] = result.reshape(2, slots, features)
@@ -377,30 +419,28 @@
             reduced[other * 2 + c] = row_sum(d, c).end().astype(BF16)
         if d == 0:
             comb[me] = reduced[me]
-            start(remote(reduced.at[twin], comb.at[me], r_send.at[0, 0], r_recv.at[0, 0], twin, part))
+            start(reduced.at[twin], comb.at[me], r_recv.at[0, 0], twin, part)
             return
         for c in range(2):
             source = other * 2 + c
-            start(remote(
-                reduced.at[source], comb.at[me], r_send.at[d, c], r_recv.at[d, core], source, part
-            ))
+            start(reduced.at[source], comb.at[me], r_recv.at[d, core], source, part)
 
     def mix_sum(h):
         return Sum(
             mix_part.at[h], mix_first.at[h], mix_pair.at[h], mix_second.at[h],
-            lambda n: m_send.at[h, n], lambda n: m_recv.at[h, n],
-            lambda n: n_send.at[h, n], lambda n: n_recv.at[h, n], h,
+            lambda n: m_recv.at[h, n], lambda n: n_recv.at[h, n], h,
         )
 
     def queries():
-        loads[0].wait()
+        for load in small[9:] + loads[:1]:
+            load.wait()
         q_normed = rms_scale(q_lat[...], q_gain[...]).astype(BF16)
         query = dot(q_normed, v_query[...])
         for h in range(heads):
             base = h * (NOPE + ROPE)
             qcat[h, :, :NOPE] = query[:, base : base + NOPE].astype(BF16)
             turn = query[:, base + NOPE : base + NOPE + ROPE].astype(BF16)
-            qcat[h, :, NOPE:] = rotate(turn, angles_q, 1)
+            qcat[h, :, NOPE:] = rotate(turn, spun[0], 1)
 
     def make_keys(d):
         first = facing(d)[1] * 2
@@ -434,6 +474,8 @@
         for h in range(2):
             result = dot(attended[...], v_mix[:, h * half : (h + 1) * half]).astype(BF16)
             mix_part[h] = result.reshape(mix_part.shape[1:])
+
+    def mix_begin():
         for h in range(2):
             mix_sum(h).begin()
 
@@ -447,70 +489,87 @@
             mixed[:, h * half : (h + 1) * half] = mix_sum(h).end().astype(BF16)
         outs[0].start()
 
-    rest = order[1:]
     for d in order[:1]:
         row_send(d)
+    prepare_latents()
+    for load in loads[1:3]:
+        load.wait()
+    row_finish(0)
+    run_expert(0)
+    sum_begin(0)
     queries()
-    for d in rest[:1]:
-        row_send(d)
     for load in loads[4:6]:
         load.wait()
     latent_twin(0)
     make_keys(0)
-    for load in loads[1:4]:
-        load.wait()
-    row_finish(0)
-    run_expert(0)
     for d in order[:1]:
         row_direct(d)
-    sum_begin(0)
-    for d in rest[1:]:
+    for d in order[1:]:
         row_send(d)
-    for d in near:
-        latent_send(d)
-    for d in rest[:1]:
-        row_direct(d)
+    sum_middle(0)
     for d in order[:1]:
         row_relay(d)
-    sum_middle(0)
+    for d in order:
+        latent_send(d)
+    for d in order[1:2]:
+        row_direct(d)
     groups = [0] + order
     last = len(order) - 1
+    pending = [functools.partial(attend, h) for h in range(heads)]
+    ended = 0
+
+    def some_heads(number):
+        for work in pending[:number]:
+            work()
+        del pending[:number]
+
     for i, d in enumerate(order):
-        if i == last:
-            for e in near:
+        row_finish(d)
+        if i + 2 <= last:
+            row_direct(order[i + 2])
+        if 0 < i < last:
+            row_relay(order[i + 1])
+        run_expert(d)
+        if i == 0 and last > 0:
+            row_relay(order[1])
+        sum_begin(d)
+        if i == max(0, last - 2):
+            for e in order:
                 latent_pass(e)
-            for e in near:
+        if i == 1:
+            sum_middle(groups[1])
+            sum_end(0)
+            ended = 1
+        if i == max(0, last - 1):
+            for e in order:
+                latent_rest(e)
+            for e in order:
                 latent_twin(e)
                 make_keys(e)
-        row_finish(d)
-        if i + 1 < last:
-            row_relay(order[i + 1])
-        if i + 2 <= last:
-            row_direct(order[i + 2])
-        run_expert(d)
-        sum_begin(d)
-        if i + 1 == last:
-            row_relay(order[last])
-        if i > 0:
+        if i == last:
+            some_heads(1)
+        if i > 1:
             sum_middle(groups[i])
-            sum_end(groups[i - 1])
-    for h in range(heads):
-        attend(h)
+            some_heads(1)
+            while ended < i:
+                sum_end(groups[ended])
+                ended += 1
+    some_heads(heads)
     make_mix()
-    for d in order[-1:]:
+    for d in groups[-1:]:
         sum_middle(d)
-    for d in groups[max(0, len(groups) - 2) : -1]:
+    mix_begin()
+    for d in groups[ended:]:
         sum_end(d)
-    sum_end(groups[-1])
     mix_middle()
     mix_end()
 
     here = comb.at[twin]
-    remote(here, here, r_send.at[0, 0], r_recv.at[0, 0], twin, part).wait_recv()
+    landed(here, r_recv.at[0, 0])
     for d in order:
         for c in range(2):
             here = comb.at[facing(d)[0] * 2 + c]
-            remote(here, here, r_send.at[d, c], r_recv.at[d, c], twin, part).wait_recv()
+            landed(here, r_recv.at[d, c])
     back = comb[...].reshape(ep_size * slots, features)
     seat = lax.broadcasted_iota(jnp.int32, (tokens, ep_size * slots), 1).astype(F32)
     result = jnp.zeros((tokens, features), F32)
@@ -519,7 +578,7 @@
         result = result + dot(pick, back) * facts[:, choose + k : choose + k + 1]
     expert_out[...] = result.astype(BF16)
     outs[1].start()
-    for copy in waits:
+    for copy in waits[-pool.shape[0] :]:
         copy.wait_send()
     for out in outs:
         out.wait()
@@ -566,6 +625,7 @@
     extent = (tp_size // narrow, narrow)
     most = max(extent)
     ahead = max(1, most - 1)
+    away = max(1, levels - 1)
     wing = width // 2
 
     lane = np.arange(128) % (ROPE // 2)
@@ -590,17 +650,22 @@
     dma = pltpu.SemaphoreType.DMA
     vmem = pl.BlockSpec(memory_space=pltpu.VMEM)
     far = pl.BlockSpec(memory_space=pl.ANY)
+    small = (
+        pad_rows(q_latent), kv_latent, rope_key.T, q_gain[None, :], kv_gain[None, :],
+        jnp.asarray(near_angle), jnp.asarray(far_angle), expert_in, norm_gain[None, :], routes.T, route_scores.T,
+    )
     mixed, expert_out = pl.pallas_call(
         functools.partial(layer_kernel, (ep_size, tp_size, slots, choose, heads, extent)),
         out_shape=(
             jax.ShapeDtypeStruct((padded, width), BF16),
             jax.ShapeDtypeStruct((tokens, features), BF16),
         ),
-        in_specs=[vmem] * 11 + [far] * 7,
+        in_specs=[far] * 18,
         out_specs=(far, far),
         scratch_shapes=[
             pltpu.VMEM((padded, width), BF16),
             pltpu.VMEM((tokens, features), BF16),
+            *[pltpu.VMEM(value.shape, value.dtype) for value in small],
             pltpu.VMEM(w_query.shape, BF16),
             pltpu.VMEM(w_key.shape, BF16),
             pltpu.VMEM(w_value.shape, BF16),
@@ -608,7 +673,7 @@
             pltpu.VMEM((width, units), BF16),
             pltpu.VMEM((width, units), BF16),
             pltpu.VMEM((units, width), BF16),
-            pltpu.VMEM((ep_size, count, kv_latent.shape[1]), BF16),
+            pltpu.VMEM((ep_size, 4, count // 4, kv_latent.shape[1]), BF16),
             pltpu.VMEM((ep_size, count // 2, 128), BF16),
             pltpu.VMEM((heads, ep_size * count, NOPE + 128), BF16),
             pltpu.VMEM((ep_size * count, heads * VDIM), BF16),
@@ -631,25 +696,17 @@
             pltpu.VMEM((ep_size, ahead, slots, features), BF16),
             pltpu.VMEM((ep_size, slots, features), BF16),
             pltpu.VMEM((ep_size, slots, features), BF16),
-            dma((9,)),
-            dma((levels, 2)), dma((levels, 2)),
-            dma((levels, 2)), dma((levels, 2)),
-            dma((2,)), dma((2,)),
-            dma((levels, 2)), dma((levels, 2)),
-            dma((levels, 2, tp_size)), dma((levels, 2, tp_size)),
-            dma((1,)), dma((1,)),
-            dma((levels, 2, ahead)), dma((levels, 2, ahead)),
-            dma((levels, 2, ahead)), dma((levels, 2, ahead)),
-            dma((levels, 2)), dma((levels, 2)),
-            dma((2, ahead)), dma((2, ahead)),
+            dma((7,)), dma((11,)), dma((32,)),
+            dma((away, 2)), dma((away, 2)), dma((away, 4)), dma((2,)),
+            dma((away, 2)), dma((away, 2, max(1, tp_size - 1))), dma((1,)),
+            dma((levels, 2, ahead)), dma((levels, 2, ahead)), dma((levels, 2)),
             dma((2, ahead)), dma((2, ahead)),
         ],
         compiler_params=pltpu.CompilerParams(
             collective_id=0, has_side_effects=True, vmem_limit_bytes=60 * 1024 * 1024
         ),
     )(
-        pad_rows(q_latent), kv_latent, rope_key.T, q_gain[None, :], kv_gain[None, :], near_angle, far_angle,
-        expert_in, norm_gain[None, :], routes.T, route_scores.T,
+        *small,
         w_query, w_key, w_value, w_mix_out, w_gate[0], w_up[0], w_down[0],
     )
     return pl.pallas_call(

time: 62.3 us -> 57.7 us (0.926)
  Pallas kernels: 61.4 us -> 56.9 us
    pallas_call x1, Pallas kernels: 59.7 us -> 55.2 us  [body(): pl.pallas_call(functools.partial(layer_kernel, (ep_size, tp_size, slots,...]
where the time goes in v3:
time: 57.7 us; the launch traced here: 57.5 us
  Pallas kernels  56.9 us (99%)
  between operations  0.65 us (1%)
    pallas_call x1, Pallas kernels, body(): pl.pallas_call(functools.partial(layer_kernel, (ep_size, tp_size, slots,...  55.2 us
    pallas_call x1, Pallas kernels, body(): pl.pallas_call(hand_over, out_shape=(jax.ShapeDtypeStruct((mine, width),...  1.74 us

profile of v3, /device:TPU:0, one launch (start us, length us, event | category | flops | bytes accessed | tf_op | source)
XLA Modules:
  0.0 57.5 jit_solution(13672783881921378919)
XLA Ops:
  0.6 55.2 %shard_map.185 = (bf16[48,2048]{1,0:T(8,128)(2,1)}, bf16[128,512]{1,0:T(8,128)(2,1)}) custom-call(bf16[192,512]{1,0:T(8,128)(2,1)} %h_q_lat.1, bf16[192,256]{1,0:T(8,128)(2,1)} %h_kv_lat.1, bf16[64,192]{1,0:T(8,128)(2,1)} %bitcast.12, f32[1,512]{1,0:T(1,128)} %bitcast.14, f32[1,256]{1,0:T(1,128)} %bitcast.15, f32[192,256]{1,0:T(8,128)} %constant.4.clone.h_near_angle, ...), custom_call_target="tpu_custom_call" | custom-call | tf_op jit(solution)/shard_map/pallas_call | solution.py:657
  55.8 1.7 %shard_map.186 = (bf16[48,2048]{1,0:T(8,128)(2,1)}, bf16[128,512]{1,0:T(8,128)(2,1)}) custom-call(bf16[48,2048]{1,0:T(8,128)(2,1)} %get-tuple-element.4.mixed_in, bf16[128,512]{1,0:T(8,128)(2,1)} %get-tuple-element.5.expert_in), custom_call_target="tpu_custom_call" | custom-call | tf_op jit(solution)/shard_map/pallas_call | solution.py:712

commit v4 on v3

--- a/solution.py
+++ b/solution.py
@@ -389,7 +389,7 @@
             lambda n: p_recv.at[d, c, n], lambda n: q_recv.at[d, c, n], c,
         )
 
-    block = min(256, v_gate.shape[1])
+    block = min(512, v_gate.shape[1])
 
     def run_expert(d):
         first = facing(d)[1] * 2
@@ -532,20 +532,21 @@
         run_expert(d)
         if i == 0 and last > 0:
             row_relay(order[1])
-        sum_begin(d)
         if i == max(0, last - 2):
             for e in order:
                 latent_pass(e)
-        if i == 1:
-            sum_middle(groups[1])
-            sum_end(0)
-            ended = 1
+        sum_begin(d)
         if i == max(0, last - 1):
             for e in order:
                 latent_rest(e)
             for e in order:
                 latent_twin(e)
                 make_keys(e)
+        if i == 1:
+            sum_middle(groups[1])
+            sum_end(0)
+            ended = 1
+            some_heads(1)
         if i == last:
             some_heads(1)
         if i > 1:
@@ -696,7 +697,7 @@
             pltpu.VMEM((ep_size, ahead, slots, features), BF16),
             pltpu.VMEM((ep_size, slots, features), BF16),
             pltpu.VMEM((ep_size, slots, features), BF16),
-            dma((7,)), dma((11,)), dma((32,)),
+            dma((7,)), dma((11,)), dma((20,)),
             dma((away, 2)), dma((away, 2)), dma((away, 4)), dma((2,)),
             dma((away, 2)), dma((away, 2, max(1, tp_size - 1))), dma((1,)),
             dma((levels, 2, ahead)), dma((levels, 2, ahead)), dma((levels, 2)),

time: 57.7 us -> 56.5 us (0.979)
  Pallas kernels: 56.9 us -> 55.7 us
    pallas_call x1, Pallas kernels: 55.2 us -> 54 us  [body(): pl.pallas_call(functools.partial(layer_kernel, (ep_size, tp_size, slots,...]
where the time goes in v4:
time: 56.5 us; the launch traced here: 56.3 us
  Pallas kernels  55.7 us (99%)
  between operations  0.65 us (1%)
    pallas_call x1, Pallas kernels, body(): pl.pallas_call(functools.partial(layer_kernel, (ep_size, tp_size, slots,...  54 us
    pallas_call x1, Pallas kernels, body(): pl.pallas_call(hand_over, out_shape=(jax.ShapeDtypeStruct((mine, width),...  1.74 us

profile of v4, /device:TPU:0, one launch (start us, length us, event | category | flops | bytes accessed | tf_op | source)
XLA Modules:
  0.0 56.3 jit_solution(10067074746724507126)
XLA Ops:
  0.6 54.0 %shard_map.185 = (bf16[48,2048]{1,0:T(8,128)(2,1)}, bf16[128,512]{1,0:T(8,128)(2,1)}) custom-call(bf16[192,512]{1,0:T(8,128)(2,1)} %h_q_lat.1, bf16[192,256]{1,0:T(8,128)(2,1)} %h_kv_lat.1, bf16[64,192]{1,0:T(8,128)(2,1)} %bitcast.12, f32[1,512]{1,0:T(1,128)} %bitcast.14, f32[1,256]{1,0:T(1,128)} %bitcast.15, f32[192,256]{1,0:T(8,128)} %constant.4.clone.h_near_angle, ...), custom_call_target="tpu_custom_call" | custom-call | tf_op jit(solution)/shard_map/pallas_call | solution.py:658
  54.6 1.7 %shard_map.186 = (bf16[48,2048]{1,0:T(8,128)(2,1)}, bf16[128,512]{1,0:T(8,128)(2,1)}) custom-call(bf16[48,2048]{1,0:T(8,128)(2,1)} %get-tuple-element.4.mixed_in, bf16[128,512]{1,0:T(8,128)(2,1)} %get-tuple-element.5.expert_in), custom_call_target="tpu_custom_call" | custom-call | tf_op jit(solution)/shard_map/pallas_call | solution.py:713

commit v5 on v4

--- a/solution.py
+++ b/solution.py
@@ -518,7 +518,11 @@
     pending = [functools.partial(attend, h) for h in range(heads)]
     ended = 0
 
+    keyed = []
+
     def some_heads(number):
+        if not keyed:
+            return
         for work in pending[:number]:
             work()
         del pending[:number]
@@ -542,6 +546,7 @@
             for e in order:
                 latent_twin(e)
                 make_keys(e)
+            keyed.append(True)
         if i == 1:
             sum_middle(groups[1])
             sum_end(0)
@@ -555,6 +560,7 @@
             while ended < i:
                 sum_end(groups[ended])
                 ended += 1
+    keyed.append(True)
     some_heads(heads)
     make_mix()
     for d in groups[-1:]:

time: 56.5 us -> 56.5 us (level)
  no operation moved by 1% of the time
where the time goes in v5:
time: 56.5 us; the launch traced here: 56.3 us
  Pallas kernels  55.7 us (99%)
  between operations  0.65 us (1%)
    pallas_call x1, Pallas kernels, body(): pl.pallas_call(functools.partial(layer_kernel, (ep_size, tp_size, slots,...  54 us
    pallas_call x1, Pallas kernels, body(): pl.pallas_call(hand_over, out_shape=(jax.ShapeDtypeStruct((mine, width),...  1.74 us

profile of v5, /device:TPU:0, one launch (start us, length us, event | category | flops | bytes accessed | tf_op | source)
XLA Modules:
  0.0 56.3 jit_solution(4509381325612971430)
XLA Ops:
  0.6 54.0 %shard_map.185 = (bf16[48,2048]{1,0:T(8,128)(2,1)}, bf16[128,512]{1,0:T(8,128)(2,1)}) custom-call(bf16[192,512]{1,0:T(8,128)(2,1)} %h_q_lat.1, bf16[192,256]{1,0:T(8,128)(2,1)} %h_kv_lat.1, bf16[64,192]{1,0:T(8,128)(2,1)} %bitcast.12, f32[1,512]{1,0:T(1,128)} %bitcast.14, f32[1,256]{1,0:T(1,128)} %bitcast.15, f32[192,256]{1,0:T(8,128)} %constant.4.clone.h_near_angle, ...), custom_call_target="tpu_custom_call" | custom-call | tf_op jit(solution)/shard_map/pallas_call | solution.py:664
  54.6 1.7 %shard_map.186 = (bf16[48,2048]{1,0:T(8,128)(2,1)}, bf16[128,512]{1,0:T(8,128)(2,1)}) custom-call(bf16[48,2048]{1,0:T(8,128)(2,1)} %get-tuple-element.4.mixed_in, bf16[128,512]{1,0:T(8,128)(2,1)} %get-tuple-element.5.expert_in), custom_call_target="tpu_custom_call" | custom-call | tf_op jit(solution)/shard_map/pallas_call | solution.py:719
